TPU v7x, 32 devices: a whole 2x2x4 slice. The times are simulated.
32 devices in a mesh: sp: 8 (over z, x), dp: 4 (over y, core).
Axes of the slice: x: 2, y: 2, z: 4, core: 2. Of those that a mesh axis runs over, the one named last changes fastest.
Arguments:
- inputs: bfloat16 [4, 2048, 2048], P('dp', 'sp'), may hold values from -6 to 6
- up_pre: bfloat16 [4, 2048, 1024], P('dp', 'sp'), may hold values from -6 to 6
- gate_pre: bfloat16 [4, 2048, 1024], P('dp', 'sp'), may hold values from -6 to 6
- cotangent: bfloat16 [4, 2048, 1024], P('dp', 'sp'), may hold values from -6 to 6
- norm_gain: float32 [1024], replicated, may hold values from 0.1 to 1.9
- up_weight: bfloat16 [2048, 1024], P('dp'), may hold values from -0.125 to 0.125
- gate_weight: bfloat16 [2048, 1024], P('dp'), may hold values from -0.125 to 0.125
- mix_weight: bfloat16 [8, 512, 512], replicated, may hold values from -0.375 to 0.375
Outputs:
- input_grad: bfloat16 [4, 2048, 2048], P('dp', 'sp')
- up_weight_grad: float32 [2048, 1024], P('dp')
- gate_weight_grad: float32 [2048, 1024], P('dp')
All inputs are finite; a program needn't handle non-finite values.
Results may differ from a plain program's by a relative error of at most 0.0064.
Values may be sent and summed in bfloat16 or wider, within the bound.
A program may use at most 128 MiB of HBM per device.

v0:
```python
import math

import jax
import jax.numpy as jnp
from jax import lax
from jax.sharding import PartitionSpec as P

GROUP_CH = 128
SPAN = 512
SEG = 64


norm_eps = 1e-05
grad_scale = 1.0 / 256.0
root_half = 1.0 / math.sqrt(2.0)
root_twopi = 1.0 / math.sqrt(2.0 * math.pi)


def gelu_value(preact):
    return 0.5 * preact * (1.0 + lax.erf(preact * root_half))


def gelu_slope(preact):
    return (
        0.5 * (1.0 + lax.erf(preact * root_half))
        + preact * jnp.exp(-0.5 * preact * preact) * root_twopi
    )


def span_mask():
    segment = jnp.arange(SPAN) // SEG
    return segment[None, :] <= segment[:, None]


def contract(first_op, second_op):
    return lax.dot_general(
        first_op, second_op, (((1,), (1,)), ((), ())), preferred_element_type=jnp.float32
    )


def on_device(inputs, up_pre, gate_pre, cotangent, norm_gain, up_weight, gate_weight, mix_weight):
    sequences, own_rows, gated_width = cotangent.shape
    model_width = inputs.shape[2]
    up_float = up_pre.astype(jnp.float32)
    gate_float = gate_pre.astype(jnp.float32)
    grad_float = cotangent.astype(jnp.float32)
    gated_act = gelu_value(gate_float)
    centered = gated_act - jnp.mean(gated_act, axis=-1, keepdims=True)
    inverse_std = lax.rsqrt(jnp.mean(centered * centered, axis=-1, keepdims=True) + norm_eps)
    normed = centered * inverse_std
    mixer_in = (normed * norm_gain).astype(jnp.bfloat16)
    mixer_grad = (grad_float * gelu_value(up_float)).astype(jnp.bfloat16)
    arrived = (
        lax.all_to_all(mixer_grad, "sp", split_axis=2, concat_axis=1, tiled=True),
        lax.all_to_all(mixer_in, "sp", split_axis=2, concat_axis=1, tiled=True),
    )
    channels = arrived[0].shape[2]
    group_index = lax.axis_index("sp") * channels // GROUP_CH
    weight_group = lax.dynamic_index_in_dim(mix_weight, group_index, 0, keepdims=False)
    masked = jnp.where(span_mask(), weight_group, jnp.zeros_like(weight_group))
    grad_blocks = arrived[0].reshape(-1, SPAN, channels)
    input_blocks = arrived[1].reshape(-1, SPAN, channels)
    spatial = jnp.einsum(
        "ts,nsc->ntc", masked, input_blocks, preferred_element_type=jnp.float32
    ).astype(jnp.bfloat16)
    normed_back = jnp.einsum(
        "ts,ntc->nsc", masked, grad_blocks, preferred_element_type=jnp.float32
    ).astype(jnp.bfloat16)
    returned = (
        lax.all_to_all(
            spatial.reshape(sequences, -1, channels), "sp", split_axis=1, concat_axis=2, tiled=True
        ),
        lax.all_to_all(
            normed_back.reshape(sequences, -1, channels),
            "sp",
            split_axis=1,
            concat_axis=2,
            tiled=True,
        ),
    )
    spatial_tokens = returned[0]
    back_tokens = returned[1]
    up_pre_grad = (grad_float * spatial_tokens.astype(jnp.float32) * gelu_slope(up_float)).astype(
        jnp.bfloat16
    )
    scaled = back_tokens.astype(jnp.float32) * norm_gain
    gated_grad = inverse_std * (
        scaled
        - jnp.mean(scaled, axis=-1, keepdims=True)
        - normed * jnp.mean(scaled * normed, axis=-1, keepdims=True)
    )
    gate_pre_grad = (gated_grad * gelu_slope(gate_float)).astype(jnp.bfloat16)
    flat_up = up_pre_grad.reshape(-1, gated_width)
    flat_gate = gate_pre_grad.reshape(-1, gated_width)
    token_count = flat_up.shape[0]
    dp_count = lax.axis_size("dp")
    sp_count = lax.axis_size("sp")
    result_part = (
        contract(flat_up, lax.all_gather(up_weight, "dp", axis=0, tiled=True))
        + contract(flat_gate, lax.all_gather(gate_weight, "dp", axis=0, tiled=True))
    ).astype(jnp.bfloat16)
    input_grad = result_part.reshape(sequences, own_rows, model_width)
    flat_inputs = inputs.reshape(-1, model_width)
    both_grads = jnp.concatenate([flat_up, flat_gate], axis=1)
    row_share = model_width // (sp_count * dp_count)
    permuted = flat_inputs.reshape(token_count, dp_count, sp_count, row_share)
    permuted = permuted.transpose(0, 2, 1, 3).reshape(token_count, model_width)
    own_part = lax.psum_scatter(
        lax.dot_general(
            permuted, both_grads, (((0,), (0,)), ((), ())), preferred_element_type=jnp.float32
        ),
        ("sp", "dp"),
        scatter_dimension=0,
        tiled=True,
    )
    weight_rows = lax.all_gather(own_part, "sp", axis=0, tiled=True)
    up_weight_grad = weight_rows[:, :gated_width] * grad_scale
    gate_weight_grad = weight_rows[:, gated_width:] * grad_scale
    return (input_grad, up_weight_grad, gate_weight_grad)


def solution(mesh):
    return jax.shard_map(
        on_device,
        mesh=mesh,
        in_specs=(
            P("dp", "sp", None),
            P("dp", "sp", None),
            P("dp", "sp", None),
            P("dp", "sp", None),
            P(),
            P("dp", None),
            P("dp", None),
            P(),
        ),
        out_specs=(P("dp", "sp", None), P("dp", None), P("dp", None)),
        check_vma=False,
    )
```

profile of v0, /device:TPU:0, one launch (start us, length us, event | category | flops | bytes accessed | tf_op | source)
XLA Modules:
  0.0 505.7 jit_solution(16661399737685429163)
XLA Ops:
  8.0 1.2 copy.45
  9.2 1.2 copy.36
  12.1 3.7 reduce.6
  16.8 7.6 %all-to-all-start.2 = ((bf16[8,2,16384]{2,1,0:T(2,128)(2,1)}), bf16[8,2,16384]{2,1,0:T(2,128)(2,1)S(1)}, u32[]{:S(2)}, u32[]{:S(2)}) async-start(bf16[8,2,16384]{2,1,0:T(2,128)(2,1)} %reshape.291), calls=%async_computation.2 | async-start | bytes 1048576 | tf_op jit(solution)/shard_map/all_to_all | solution.py:54
  24.4 14.4 %all-to-all-done.2 = bf16[8,2,16384]{2,1,0:T(2,128)(2,1)S(1)} async-done(((bf16[8,2,16384]{2,1,0:T(2,128)(2,1)}), bf16[8,2,16384]{2,1,0:T(2,128)(2,1)S(1)}, u32[]{:S(2)}, u32[]{:S(2)}) %all-to-all-start.2) | async-done | bytes 524320 | tf_op jit(solution)/shard_map/all_to_all | solution.py:54
  39.8 1.6 fusion.3
  41.7 8.1 %copy.67 = bf16[1,2048,128]{2,0,1:T(2,128)(2,1)S(1)} copy(bf16[1,2048,128]{2,1,0:T(8,128)(2,1)S(1)} %bitcast.88) | data formatting | bytes 1048576 | tf_op jit(solution)/shard_map/reshape | solution.py:74
  49.8 11.4 %reduce.7 = bf16[2048,128]{1,0:T(8,128)(2,1)S(1)} reduce(bf16[2048,1,128]{2,1,0:T(2,128)(2,1)S(1)} %bitcast.80, bf16[]{:T(256)} %broadcast.266), dimensions={1}, to_apply=%bitcast.69.reduce_sub_computation | reduce | bytes 1048578
  62.2 4.7 all-to-all-start.3
  67.6 13.5 %all-to-all-done.3 = bf16[8,2,16384]{2,1,0:T(2,128)(2,1)} async-done(((bf16[8,2,16384]{2,1,0:T(2,128)(2,1)}), bf16[8,2,16384]{2,1,0:T(2,128)(2,1)}, u32[]{:S(2)}, u32[]{:S(2)}) %all-to-all-start.3) | async-done | bytes 524320 | tf_op jit(solution)/shard_map/all_to_all | solution.py:73
  81.1 2.2 reshape.294
  83.4 1.3 convert_bitcast_fusion
  84.6 1.6 copy.52
  86.2 1.2 fusion.7
  87.8 1.5 fusion.15
  90.1 3.7 reduce.8
  94.0 18.2 %all_to_all.48 = bf16[8,2,16384]{2,1,0:T(2,128)(2,1)S(1)} all-to-all(bf16[8,2,16384]{2,1,0:T(2,128)(2,1)S(1)} %reshape.287), channel_id=1, replica_groups=mesh['sp'=8,'dp'=4] {'sp'}, dimensions={0} | all-to-all | bytes 1048576 | tf_op jit(solution)/shard_map/all_to_all | solution.py:55
  113.1 1.6 fusion.2
  115.0 8.1 %copy.69 = bf16[1,2048,128]{2,0,1:T(2,128)(2,1)S(1)} copy(bf16[1,2048,128]{2,1,0:T(8,128)(2,1)S(1)} %bitcast.90) | data formatting | bytes 1048576 | tf_op jit(solution)/shard_map/reshape | solution.py:71
  123.1 11.4 %reduce.9 = bf16[2048,128]{1,0:T(8,128)(2,1)S(1)} reduce(bf16[2048,1,128]{2,1,0:T(2,128)(2,1)S(1)} %bitcast.79, bf16[]{:T(256)} %broadcast.266), dimensions={1}, to_apply=%bitcast.71.reduce_sub_computation | reduce | bytes 1048578
  135.5 4.1 all-to-all-start.1
  139.9 1.5 copy.53
  141.5 11.9 %all-to-all-done.1 = bf16[8,2,16384]{2,1,0:T(2,128)(2,1)} async-done(((bf16[8,2,16384]{2,1,0:T(2,128)(2,1)}), bf16[8,2,16384]{2,1,0:T(2,128)(2,1)}, u32[]{:S(2)}, u32[]{:S(2)}) %all-to-all-start.1) | async-done | bytes 524320 | tf_op jit(solution)/shard_map/all_to_all | solution.py:70
  153.4 2.2 reshape.290
  156.7 1.6 copy.44
  159.6 9.1 %convolution_bitcast_fusion = f32[2048,2048]{0,1:T(8,128)} fusion(bf16[256,2048]{0,1:T(8,128)(2,1)S(1)} %bitcast.73, bf16[256,1024]{0,1:T(8,128)(2,1)} %bitcast.83, bf16[256,1024]{0,1:T(8,128)(2,1)S(1)} %bitcast.84), kind=kOutput, calls=%fused_computation | convolution fusion | flops 2149580800 | bytes 18874368 | tf_op jit(solution)/shard_map/dot_general | solution.py:109
  168.8 17.6 %copy.58 = f32[2048,2048]{1,0:T(8,128)} copy(f32[2048,2048]{0,1:T(8,128)} %convolution_bitcast_fusion) | data formatting | bytes 33554432
  187.6 231.8 %reduce-scatter.4.cloned.1.call-done = f32[64,2048]{1,0:T(8,128)} async-done(((f32[2048,2048]{1,0:T(8,128)}), f32[64,2048]{1,0:T(8,128)}) %reduce-scatter.4.cloned.1.call-update) | async-done | bytes 524304 | tf_op jit(solution)/shard_map/reduce_scatter | solution.py:108
  419.5 3.5 fusion.36
  423.0 4.5 fusion.1
  427.5 65.3 %all-gather.8.cloned.1.call-done = f32[512,2048]{1,0:T(8,128)} async-done(((f32[64,2048]{1,0:T(8,128)}), f32[512,2048]{1,0:T(8,128)}) %all-gather.8.cloned.1.call-update) | async-done | bytes 4194320 | tf_op jit(solution)/shard_map/all_gather | solution.py:116
  492.8 5.1 %slice_multiply_fusion = (f32[512,1024]{1,0:T(8,128)}, f32[512,1024]{1,0:T(8,128)}) fusion(f32[512,2048]{1,0:T(8,128)} %all-gather.8.cloned.1.call-done), kind=kLoop, calls=%fused_computation.4 | loop fusion | flops 1048576 | bytes 8388608 | tf_op jit(solution)/shard_map/mul | solution.py:118
  (52 shorter events, 12.7 us)
Async XLA Ops:
  10.5 28.9 %copy-start = (bf16[1,256,1024]{1,2,0:T(8,128)(2,1)}, bf16[1,256,1024]{1,2,0:T(8,128)(2,1)S(1)}, u32[]{:S(2)}) copy-start(bf16[1,256,1024]{1,2,0:T(8,128)(2,1)S(1)} %copy.36) | copy-start | bytes 1572868
  16.8 22.0 %all-to-all-start.2 = ((bf16[8,2,16384]{2,1,0:T(2,128)(2,1)}), bf16[8,2,16384]{2,1,0:T(2,128)(2,1)S(1)}, u32[]{:S(2)}, u32[]{:S(2)}) async-start(bf16[8,2,16384]{2,1,0:T(2,128)(2,1)} %reshape.291), calls=%async_computation.2 | async-start | bytes 1048576 | tf_op jit(solution)/shard_map/all_to_all | solution.py:54
  39.8 27.1 %copy-start.5 = (bf16[1,256,1024]{2,1,0:T(8,128)(2,1)S(1)}, bf16[1,256,1024]{2,1,0:T(8,128)(2,1)}, u32[]{:S(2)}) copy-start(bf16[1,256,1024]{2,1,0:T(8,128)(2,1)} %param.10) | copy-start | bytes 1572868
  62.2 18.9 %all-to-all-start.3 = ((bf16[8,2,16384]{2,1,0:T(2,128)(2,1)}), bf16[8,2,16384]{2,1,0:T(2,128)(2,1)}, u32[]{:S(2)}, u32[]{:S(2)}) async-start(bf16[8,2,16384]{2,1,0:T(2,128)(2,1)} %reshape.293), calls=%async_computation.3 | async-start | bytes 1048576 | tf_op jit(solution)/shard_map/all_to_all | solution.py:73
  67.4 18.8 %copy-start.6 = (f32[1024]{0:T(1024)S(1)}, f32[1024]{0:T(1024)}, u32[]{:S(2)}) copy-start(f32[1024]{0:T(1024)} %param.12) | copy-start | bytes 12292
  135.5 17.9 %all-to-all-start.1 = ((bf16[8,2,16384]{2,1,0:T(2,128)(2,1)}), bf16[8,2,16384]{2,1,0:T(2,128)(2,1)}, u32[]{:S(2)}, u32[]{:S(2)}) async-start(bf16[8,2,16384]{2,1,0:T(2,128)(2,1)} %reshape.289), calls=%async_computation.1 | async-start | bytes 1048576 | tf_op jit(solution)/shard_map/all_to_all | solution.py:70
  139.6 279.8 %reduce-scatter.4.cloned.1.call-start = ((), (), s32[]{:S(2)}) async-start(), calls=%async_computation.8 | async-start | bytes 17301504 | tf_op jit(solution)/shard_map/reduce_scatter | solution.py:108
  141.4 16.9 %copy-start.1 = (bf16[1,256,1024]{1,2,0:T(8,128)(2,1)S(1)}, bf16[1,256,1024]{1,2,0:T(8,128)(2,1)}, u32[]{:S(2)}) copy-start(bf16[1,256,1024]{1,2,0:T(8,128)(2,1)} %copy-done) | copy-start | bytes 1572868
  158.8 0.8 copy-start.3
  186.4 233.1 %copy-start.4 = (bf16[1,256,1024]{1,2,0:T(8,128)(2,1)S(1)}, bf16[1,256,1024]{1,2,0:T(8,128)(2,1)}, u32[]{:S(2)}) copy-start(bf16[1,256,1024]{1,2,0:T(8,128)(2,1)} %copy-done.3) | copy-start | bytes 1572868
  186.4 233.1 %all-gather.4.cloned.1.call-start = ((), (), s32[]{:S(2)}) async-start(), calls=%async_computation.5 | async-start | bytes 5242880 | tf_op jit(solution)/shard_map/all_gather | solution.py:99
  187.0 236.0 %copy-start.2 = (bf16[1,256,1024]{1,2,0:T(8,128)(2,1)S(1)}, bf16[1,256,1024]{1,2,0:T(8,128)(2,1)}, u32[]{:S(2)}) copy-start(bf16[1,256,1024]{1,2,0:T(8,128)(2,1)} %get-tuple-element.18) | copy-start | bytes 1572868
  187.0 236.0 %all-gather.6.cloned.1.call-start = ((), (), s32[]{:S(2)}) async-start(), calls=%async_computation.6 | async-start | bytes 5242880 | tf_op jit(solution)/shard_map/all_gather | solution.py:100
  187.6 305.2 %all-gather.8.cloned.1.call-start = ((), (), s32[]{:S(2)}) async-start(), calls=%async_computation.7 | async-start | bytes 4718592 | tf_op jit(solution)/shard_map/all_gather | solution.py:116
Sparse Core Ops, SparseCore 0:
  186.5 232.8 reduce-scatter.3
Sparse Core Ops, SparseCore 1:
  188.4 42.2 all-gather.3
  232.1 41.9 all-gather.5
  419.5 73.2 all-gather.7
where the time goes:
time: 511 us; the launch traced here: 506 us
  waiting for transfers between devices  338 us (66%)
  local copies, waits for them, and re-layouts  53.9 us (11%)
  other arithmetic  42.2 us (8%)
  matrix products  20.4 us (4%)
  blocking collectives  18.2 us (4%)
  starting transfers between devices  16.8 us (3%)
  between operations  16.3 us (3%)
    reduce_scatter x1, waiting for transfers between devices, on_device(): lax.psum_scatter(lax.dot_general(permuted, both_grads, (((0,), (0,)), (()...  232 us
    all_gather x1, waiting for transfers between devices, on_device(): weight_rows = lax.all_gather(own_part, 'sp', axis=0, tiled=True)  65.3 us
    unnamed x30, local copies, waits for them, and re-layouts  31.6 us
    unnamed x4, other arithmetic  30.4 us
    all_to_all x1, blocking collectives, on_device(): lax.all_to_all(mixer_in, 'sp', split_axis=2, concat_axis=1, tiled=True)  18.2 us
    all_to_all x1, waiting for transfers between devices, on_device(): lax.all_to_all(mixer_grad, 'sp', split_axis=2, concat_axis=1, tiled=True)  14.4 us
    all_to_all x1, waiting for transfers between devices, on_device(): lax.all_to_all(normed_back.reshape(sequences, -1, channels), 'sp', split_...  13.5 us
    all_to_all x1, waiting for transfers between devices, on_device(): lax.all_to_all(spatial.reshape(sequences, -1, channels), 'sp', split_axis...  11.9 us
  transfers between devices with their start and end apart: 7, of which 5 were waited for; matrix products, arithmetic and copies ran while one was open for 2% of the time, Pallas kernels for 0%

commit v1 on v0

v1 whole, which is shorter than its diff:
```python
import math

import jax
import jax.numpy as jnp
from jax import lax
from jax.sharding import PartitionSpec as P

GROUP_CH = 128
SPAN = 512
SEG = 64


norm_eps = 1e-05
grad_scale = 1.0 / 256.0
root_half = 1.0 / math.sqrt(2.0)
root_twopi = 1.0 / math.sqrt(2.0 * math.pi)


def gelu_value(preact):
    return 0.5 * preact * (1.0 + lax.erf(preact * root_half))


def gelu_slope(preact):
    return (
        0.5 * (1.0 + lax.erf(preact * root_half))
        + preact * jnp.exp(-0.5 * preact * preact) * root_twopi
    )


def contract(first_op, second_op, first_dim, second_dim):
    return lax.dot_general(
        first_op,
        second_op,
        (((first_dim,), (second_dim,)), ((), ())),
        preferred_element_type=jnp.float32,
    )


def on_device(inputs, up_pre, gate_pre, cotangent, norm_gain, up_weight, gate_weight, mix_weight):
    sequences, own_rows, gated_width = cotangent.shape
    model_width = inputs.shape[2]
    sp_count = lax.axis_size("sp")
    assert sequences == 1 and own_rows * 2 == SPAN
    groups = gated_width // GROUP_CH
    input_columns = lax.all_to_all(inputs[0], "dp", split_axis=1, concat_axis=0, tiled=True)
    up_float = up_pre[0].astype(jnp.float32)
    gate_float = gate_pre[0].astype(jnp.float32)
    grad_float = cotangent[0].astype(jnp.float32)
    gated_act = gelu_value(gate_float)
    centered = gated_act - jnp.mean(gated_act, axis=-1, keepdims=True)
    inverse_std = lax.rsqrt(jnp.mean(centered * centered, axis=-1, keepdims=True) + norm_eps)
    normed = centered * inverse_std
    mixer_in = (normed * norm_gain).astype(jnp.bfloat16)
    mixer_grad = (grad_float * gelu_value(up_float)).astype(jnp.bfloat16)
    half = lax.axis_index("sp") % 2
    arrived = lax.ppermute(
        jnp.where(half == 0, mixer_in, mixer_grad), "sp", [(i, i ^ 1) for i in range(sp_count)]
    )
    segment = jnp.arange(own_rows) // SEG
    own_block = lax.dynamic_slice(
        mix_weight, (0, half * own_rows, half * own_rows), (groups, own_rows, own_rows)
    )
    own_block = jnp.where(
        segment[None, :] <= segment[:, None], own_block, jnp.zeros_like(own_block)
    )
    cross_block = mix_weight[:, own_rows:, :own_rows]
    cross_block = jnp.where(half == 0, cross_block.transpose(0, 2, 1), cross_block)
    shape = (own_rows, groups, GROUP_CH)
    own_in = mixer_in.reshape(shape)
    own_grad = mixer_grad.reshape(shape)
    f32 = jnp.float32
    cross = jnp.einsum("gts,sgc->tgc", cross_block, arrived.reshape(shape), preferred_element_type=f32)
    spatial = jnp.einsum("gts,sgc->tgc", own_block, own_in, preferred_element_type=f32)
    back = jnp.einsum("gts,tgc->sgc", own_block, own_grad, preferred_element_type=f32)
    flat = (own_rows, gated_width)
    spatial = (spatial + jnp.where(half == 0, 0.0, cross)).astype(jnp.bfloat16).reshape(flat)
    back = (back + jnp.where(half == 0, cross, 0.0)).astype(jnp.bfloat16).reshape(flat)
    up_pre_grad = (grad_float * spatial.astype(f32) * gelu_slope(up_float)).astype(jnp.bfloat16)
    scaled = back.astype(f32) * norm_gain
    gated_grad = inverse_std * (
        scaled
        - jnp.mean(scaled, axis=-1, keepdims=True)
        - normed * jnp.mean(scaled * normed, axis=-1, keepdims=True)
    )
    gate_pre_grad = (gated_grad * gelu_slope(gate_float)).astype(jnp.bfloat16)
    both_grads = jnp.concatenate([up_pre_grad, gate_pre_grad], axis=1)
    all_grads = lax.all_gather(both_grads, "dp", axis=0, tiled=True)
    weight_part = contract(input_columns, all_grads, 0, 0).astype(jnp.bfloat16)
    own_part = lax.psum_scatter(weight_part, "sp", scatter_dimension=0, tiled=True)
    weight_rows = lax.all_gather(own_part, "sp", axis=0, tiled=True).astype(f32)
    both_weights = jnp.concatenate([up_weight, gate_weight], axis=1)
    result_part = contract(all_grads, both_weights, 1, 1).astype(jnp.bfloat16)
    input_grad = lax.all_to_all(result_part, "dp", split_axis=0, concat_axis=1, tiled=True)
    up_weight_grad = weight_rows[:, :gated_width] * grad_scale
    gate_weight_grad = weight_rows[:, gated_width:] * grad_scale
    return (input_grad[None], up_weight_grad, gate_weight_grad)


def solution(mesh):
    return jax.shard_map(
        on_device,
        mesh=mesh,
        in_specs=(
            P("dp", "sp", None),
            P("dp", "sp", None),
            P("dp", "sp", None),
            P("dp", "sp", None),
            P(),
            P("dp", None),
            P("dp", None),
            P(),
        ),
        out_specs=(P("dp", "sp", None), P("dp", None), P("dp", None)),
        check_vma=False,
    )
```

time: 511 us -> 227 us (0.44)
  waiting for transfers between devices: 338 us -> 117 us
  local copies, waits for them, and re-layouts: 53.9 us -> 17 us
  other arithmetic: 42.2 us -> 17.6 us
  blocking collectives: 18.2 us -> 40.6 us
  starting transfers between devices: 16.8 us -> 3.09 us
    reduce_scatter x1, waiting for transfers between devices: 232 us -> 68.7 us  [on_device(): lax.psum_scatter(weight_part, 'sp', scatter_dimension=0, tiled=True)]
    all_to_all x3 -> x0, waiting for transfers between devices: 39.8 us -> none  [the longest x1 14.4 us: on_device(): lax.all_to_all(mixer_grad, 'sp', split_axis=2, concat_axis=1, tiled=True)]
    unnamed x4 -> x0, other arithmetic: 30.4 us -> none
    unnamed x30 -> x20, local copies, waits for them, and re-layouts: 31.6 us -> 2.95 us
    all_to_all x1 -> x2, blocking collectives: 18.2 us -> 40.6 us  [the longest x1 23.6 us: on_device(): lax.all_to_all(inputs[0], 'dp', split_axis=1, concat_axis=0, tiled=True)]
    all_gather x3 -> x2, waiting for transfers between devices: 65.4 us -> 43.2 us  [the longest x1 26 us: on_device(): weight_rows = lax.all_gather(own_part, 'sp', axis=0, tiled=True).astype(f32)]
    all_to_all x3 -> x0, starting transfers between devices: 16.4 us -> none  [the longest x1 7.6 us: on_device(): lax.all_to_all(mixer_grad, 'sp', split_axis=2, concat_axis=1, tiled=True)]
    reshape x2 -> x0, local copies, waits for them, and re-layouts: 16.3 us -> none  [the longest x1 8.14 us: on_device(): normed_back.reshape(sequences, -1, channels)]
  transfers between devices with their start and end apart: 7 -> 4, of which waited for: 5 -> 4; matrix products, arithmetic and copies ran while one was open for 2% -> 7% of each run, Pallas kernels for 0% -> 0%
where the time goes in v1:
time: 227 us
  waiting for transfers between devices  117 us (52%)
  blocking collectives  40.6 us (18%)
  other arithmetic  17.6 us (8%)
  matrix products  17.1 us (8%)
  local copies, waits for them, and re-layouts  17 us (7%)
  between operations  13.9 us (6%)
  starting transfers between devices  3.09 us (1%)
    reduce_scatter x1, waiting for transfers between devices, on_device(): lax.psum_scatter(weight_part, 'sp', scatter_dimension=0, tiled=True)  68.7 us
    all_gather x1, waiting for transfers between devices, on_device(): weight_rows = lax.all_gather(own_part, 'sp', axis=0, tiled=True).astype(f32)  26 us
    all_to_all x1, blocking collectives, on_device(): lax.all_to_all(inputs[0], 'dp', split_axis=1, concat_axis=0, tiled=True)  23.6 us
    all_gather x1, waiting for transfers between devices, on_device(): all_grads = lax.all_gather(both_grads, 'dp', axis=0, tiled=True)  17.2 us
    all_to_all x1, blocking collectives, on_device(): lax.all_to_all(result_part, 'dp', split_axis=0, concat_axis=1, tiled=True)  17 us
    dot_general x2, matrix products, contract(): lax.dot_general(first_op, second_op, (((first_dim,), (second_dim,)), ((),...  9.41 us
    ppermute x1, waiting for transfers between devices, on_device(): lax.ppermute(jnp.where(half == 0, mixer_in, mixer_grad), 'sp', [(i, i ^ 1...  5.4 us
  transfers between devices with their start and end apart: 4, of which 4 were waited for; matrix products, arithmetic and copies ran while one was open for 7% of the time, Pallas kernels for 0%

profile of v1, /device:TPU:0, one launch (start us, length us, event | category | flops | bytes accessed | tf_op | source)
XLA Modules:
  0.0 226.7 jit_solution(4950640529958930005)
XLA Ops:
  7.2 1.4 fusion.49
  8.7 1.3 multiply_reduce_fusion
  10.0 2.7 %fusion.50 = bf16[256,1024]{1,0:T(8,128)(2,1)} fusion(f32[256,1024]{1,0:T(8,128)S(1)} %get-tuple-element.13, bf16[1,256,1024]{2,1,0:T(8,128)(2,1)} %param.10, bf16[1,256,1024]{2,1,0:T(8,128)(2,1)} %param.9, bf16[1,256,1024]{2,1,0:T(8,128)(2,1)} %param.11, f32[1024]{0:T(1024)} %param.12, f32[256]{0:T(256)S(1)} %add_rsqrt_fusion, ...), kind=kLoop, calls=%fused_computation.71 | loop fusion | flops 4194304 | bytes 3151873 | tf_op jit(solution)/shard_map/jit(_where)/select_n | solution.py:57
  12.7 3.0 %collective-permute-start = (bf16[256,1024]{1,0:T(8,128)(2,1)}, bf16[256,1024]{1,0:T(8,128)(2,1)}, u32[]{:S(2)}, u32[]{:S(2)}) collective-permute-start(bf16[256,1024]{1,0:T(8,128)(2,1)} %fusion.50), channel_id=1, source_target_pairs={{0,4},{4,0},{8,12},{12,8},{16,20},{20,16},{24,28},{28,24},{1,5},{5... | collective-permute-start | bytes 1572872 | tf_op jit(solution)/shard_map/ppermute | solution.py:56
  16.0 1.0 copy.50
  17.0 1.3 slice.9
  18.3 1.3 copy.42
  19.7 1.2 fusion.29
  20.8 1.6 copy.40
  22.5 5.4 %collective-permute-done = bf16[256,1024]{1,0:T(8,128)(2,1)} collective-permute-done((bf16[256,1024]{1,0:T(8,128)(2,1)}, bf16[256,1024]{1,0:T(8,128)(2,1)}, u32[]{:S(2)}, u32[]{:S(2)}) %collective-permute-start) | collective-permute-done | bytes 524320 | tf_op jit(solution)/shard_map/ppermute | solution.py:56
  27.9 2.0 copy.41
  30.0 2.2 fusion.43
  32.2 2.7 %fusion.47 = f32[8,128,256]{2,1,0:T(8,128)} fusion(f32[8,128,256]{2,1,0:T(8,128)S(1)} %fusion.43, bf16[8,512,512]{2,1,0:T(8,128)(2,1)} %param.15, s32[]{:T(128)S(6)} %select_n.62, pred[256,256]{1,0:T(8,128)(4,1)S(1)} %broadcast_compare_fusion, f32[256,8,128]{0,2,1:T(8,128)S(1)} %bitcast.121, f32[8,128]{1,0:T(8,128)S(1)} %bitcast.132, ...), kind=kOutput, calls=%fused_computation.68 | convolution fusion | flops 136839168 | bytes 4265989 | tf_op jit(solution)/shard_map/gts,sgc->tgc/dot_general | solution.py:73
  35.0 2.7 %fusion.42 = (f32[256]{0:T(256)S(1)}, f32[8,128,256]{2,1,0:T(8,128)}) fusion(f32[256,8,128]{0,2,1:T(8,128)S(1)} %bitcast.122, f32[8,128]{1,0:T(8,128)S(1)} %bitcast.133, f32[256]{0:T(256)S(1)} %add_rsqrt_fusion, f32[256]{0:T(256)S(1)} %broadcast_multiply_fusion.2, f32[8,128,256]{2,1,0:T(8,128)S(1)} %fusion.43, pred[]{:T(512)S(6)} %eq.4, ...), kind=kOutput, calls=%fused_computation.54 | convolution fusion | flops 137101056 | bytes 4791301 | tf_op jit(solution)/shard_map/gts,tgc->sgc/dot_general | solution.py:74
  37.7 2.6 %copy.43 = f32[256,1024]{1,0:T(8,128)} copy(f32[256,1024]{0,1:T(8,128)} %bitcast.124) | data formatting | bytes 2097152 | tf_op jit(solution)/shard_map/convert_element_type | solution.py:78
  40.3 2.7 %fusion.20 = bf16[256,1024]{1,0:T(8,128)(2,1)} fusion(f32[256,1024]{1,0:T(8,128)} %copy.43, bf16[1,256,1024]{2,1,0:T(8,128)(2,1)} %param.11, bf16[1,256,1024]{2,1,0:T(8,128)(2,1)S(1)} %copy-done.2), kind=kLoop, calls=%fused_computation.30 | loop fusion | flops 3407872 | bytes 2621440 | tf_op jit(solution)/shard_map/convert_element_type | solution.py:78
  43.2 1.3 copy.45
  44.5 2.0 fusion.28
  46.5 1.1 pad_maximum_fusion
  48.2 23.6 %all_to_all.35 = bf16[256,4,512]{0,2,1:T(8,128)(2,1)S(1)} all-to-all(bf16[256,4,512]{0,2,1:T(8,128)(2,1)S(1)} %bitcast.127), channel_id=1, replica_groups=mesh['sp'=8,'dp'=4] {'dp'}, dimensions={1} | all-to-all | bytes 2097152 | tf_op jit(solution)/shard_map/all_to_all | solution.py:45
  71.8 0.5 copy.48
  72.4 17.2 %all-gather.3.cloned.1.call-done = bf16[1024,2048]{1,0:T(8,128)(2,1)} async-done(((bf16[256,2048]{1,0:T(8,128)(2,1)}), bf16[1024,2048]{1,0:T(8,128)(2,1)}) %all-gather.3.cloned.1.call-update) | async-done | bytes 4194320 | tf_op jit(solution)/shard_map/all_gather | solution.py:87
  89.6 4.6 %fusion = bf16[512,2048]{0,1:T(8,128)(2,1)S(1)} fusion(bf16[1024,2048]{1,0:T(8,128)(2,1)} %all-gather.3.cloned.1.call-done, bf16[1024,512]{1,0:T(8,128)(2,1)S(1)} %bitcast.130), kind=kOutput, calls=%fused_computation.1 | convolution fusion | flops 2148532224 | bytes 7340032 | tf_op jit(solution)/shard_map/dot_general | solution.py:31
  94.1 2.4 %copy.51 = bf16[512,2048]{1,0:T(8,128)(2,1)} copy(bf16[512,2048]{0,1:T(8,128)(2,1)S(1)} %fusion) | data formatting | bytes 4194304
  96.6 68.7 %reduce-scatter.4.cloned.1.call-done = bf16[64,2048]{1,0:T(8,128)(2,1)} async-done(((bf16[512,2048]{1,0:T(8,128)(2,1)}), bf16[64,2048]{1,0:T(8,128)(2,1)}) %reduce-scatter.4.cloned.1.call-update) | async-done | bytes 262160 | tf_op jit(solution)/shard_map/reduce_scatter | solution.py:89
  165.4 4.8 %fusion.13 = bf16[1024,512]{1,0:T(8,128)(2,1)S(1)} fusion(bf16[1024,2048]{1,0:T(8,128)(2,1)} %all-gather.3.cloned.1.call-done, bf16[512,1024]{1,0:T(8,128)(2,1)S(1)} %copy-done.8, bf16[512,1024]{1,0:T(8,128)(2,1)} %param.13), kind=kOutput, calls=%fused_computation.23 | convolution fusion | flops 2152202240 | bytes 7340032 | tf_op jit(solution)/shard_map/dot_general | solution.py:31
  170.2 17.0 %all_to_all.36 = bf16[4,256,512]{2,1,0:T(8,128)(2,1)S(1)} all-to-all(bf16[4,256,512]{2,1,0:T(8,128)(2,1)S(1)} %bitcast.131), channel_id=1, replica_groups=mesh['sp'=8,'dp'=4] {'dp'}, dimensions={0} | all-to-all | bytes 2097152 | tf_op jit(solution)/shard_map/all_to_all | solution.py:93
  187.2 0.8 copy.46
  188.0 1.6 broadcast_in_dim.27
  189.6 26.0 %all-gather.5.cloned.1.call-done = bf16[512,2048]{1,0:T(8,128)(2,1)} async-done(((bf16[64,2048]{1,0:T(8,128)(2,1)}), bf16[512,2048]{1,0:T(8,128)(2,1)}) %all-gather.5.cloned.1.call-update) | async-done | bytes 2097168 | tf_op jit(solution)/shard_map/all_gather | solution.py:90
  215.6 2.1 convert_element_type.122
  217.7 2.5 %slice_multiply_fusion = (f32[512,1024]{1,0:T(8,128)}, f32[512,1024]{1,0:T(8,128)}) fusion(f32[512,2048]{1,0:T(8,128)S(1)} %convert_element_type.122), kind=kLoop, calls=%fused_computation.2 | loop fusion | flops 1048576 | bytes 8388608 | tf_op jit(solution)/shard_map/mul | solution.py:95
  (32 shorter events, 1.4 us)
Async XLA Ops:
  7.2 8.5 %copy-start.3 = (bf16[1,256,1024]{2,1,0:T(8,128)(2,1)S(1)}, bf16[1,256,1024]{2,1,0:T(8,128)(2,1)}, u32[]{:S(2)}) copy-start(bf16[1,256,1024]{2,1,0:T(8,128)(2,1)} %param.11) | copy-start | bytes 1572868
  7.2 8.5 %copy-start.2 = (bf16[1,256,1024]{2,1,0:T(8,128)(2,1)S(1)}, bf16[1,256,1024]{2,1,0:T(8,128)(2,1)}, u32[]{:S(2)}) copy-start(bf16[1,256,1024]{2,1,0:T(8,128)(2,1)} %param.9) | copy-start | bytes 1572868
  7.2 82.4 %all-gather.3.cloned.1.call-start = ((), (), s32[]{:S(2)}) async-start(), calls=%async_computation.3 | async-start | bytes 5242880 | tf_op jit(solution)/shard_map/all_gather | solution.py:87
  12.7 6.9 %copy-start = (bf16[1,256,1024]{2,1,0:T(8,128)(2,1)S(1)}, bf16[1,256,1024]{2,1,0:T(8,128)(2,1)}, u32[]{:S(2)}) copy-start(bf16[1,256,1024]{2,1,0:T(8,128)(2,1)} %param.10) | copy-start | bytes 1572868
  12.7 15.2 %collective-permute-start = (bf16[256,1024]{1,0:T(8,128)(2,1)}, bf16[256,1024]{1,0:T(8,128)(2,1)}, u32[]{:S(2)}, u32[]{:S(2)}) collective-permute-start(bf16[256,1024]{1,0:T(8,128)(2,1)} %fusion.50), channel_id=1, source_target_pairs={{0,4},{4,0},{8,12},{12,8},{16,20},{20,16},{24,28},{28,24},{1,5},{5... | collective-permute-start | bytes 1572872 | tf_op jit(solution)/shard_map/ppermute | solution.py:56
  19.7 12.6 %copy-start.7 = (f32[1024]{0:T(1024)S(1)}, f32[1024]{0:T(1024)}, u32[]{:S(2)}) copy-start(f32[1024]{0:T(1024)} %param.12) | copy-start | bytes 12292
  30.0 5.0 %copy-start.4 = (bf16[1,256,1024]{1,2,0:T(8,128)(2,1)S(1)}, bf16[1,256,1024]{1,2,0:T(8,128)(2,1)}, u32[]{:S(2)}) copy-start(bf16[1,256,1024]{1,2,0:T(8,128)(2,1)} %copy.50) | copy-start | bytes 1572868
  37.7 5.3 %copy-start.1 = (f32[8,128,256]{2,1,0:T(8,128)S(1)}, f32[8,128,256]{2,1,0:T(8,128)}, u32[]{:S(2)}) copy-start(f32[8,128,256]{2,1,0:T(8,128)} %get-tuple-element.17) | copy-start | bytes 3145732
  43.0 3.5 %copy-start.5 = (bf16[256,1024]{1,0:T(8,128)(2,1)S(1)}, bf16[256,1024]{1,0:T(8,128)(2,1)}, u32[]{:S(2)}) copy-start(bf16[256,1024]{1,0:T(8,128)(2,1)} %fusion.20) | copy-start | bytes 1572868
  44.5 3.1 %copy-start.6 = (bf16[1,256,2048]{2,1,0:T(8,128)(2,1)S(1)}, bf16[1,256,2048]{2,1,0:T(8,128)(2,1)}, u32[]{:S(2)}) copy-start(bf16[1,256,2048]{2,1,0:T(8,128)(2,1)} %param.8) | copy-start | bytes 3145732
  47.6 117.7 %reduce-scatter.4.cloned.1.call-start = ((), (), s32[]{:S(2)}) async-start(), calls=%async_computation.5 | async-start | bytes 2359296 | tf_op jit(solution)/shard_map/reduce_scatter | solution.py:89
  94.1 71.2 %copy-start.8 = (bf16[512,1024]{1,0:T(8,128)(2,1)S(1)}, bf16[512,1024]{1,0:T(8,128)(2,1)}, u32[]{:S(2)}) copy-start(bf16[512,1024]{1,0:T(8,128)(2,1)} %param.14) | copy-start | bytes 3145732
  96.5 119.1 %all-gather.5.cloned.1.call-start = ((), (), s32[]{:S(2)}) async-start(), calls=%async_computation.4 | async-start | bytes 2359296 | tf_op jit(solution)/shard_map/all_gather | solution.py:90
Sparse Core Ops, SparseCore 0:
  47.7 41.7 all-gather.2
  96.7 68.6 reduce-scatter.3
  167.5 48.0 all-gather.4

commit v2 on v1

--- a/solution.py
+++ b/solution.py
@@ -1,8 +1,11 @@
+import functools
 import math
 
 import jax
 import jax.numpy as jnp
 from jax import lax
+from jax.experimental import pallas as pl
+from jax.experimental.pallas import tpu as pltpu
 from jax.sharding import PartitionSpec as P
 
 GROUP_CH = 128
@@ -27,13 +30,209 @@
     )
 
 
-def contract(first_op, second_op, first_dim, second_dim):
-    return lax.dot_general(
-        first_op,
-        second_op,
-        (((first_dim,), (second_dim,)), ((), ())),
-        preferred_element_type=jnp.float32,
-    )
+CHUNKS = 4
+MESH = pl.DeviceIdType.MESH
+
+
+def exchange_kernel(
+    sizes, grads, columns, up_weight, gate_weight, sums, pieces,
+    held, partial, x_arrived, x_sum, z_arrived, result,
+    g_send, g_recv, x_send, x_recv, z_send, z_recv,
+    az_send, az_recv, ax_send, ax_recv, r_send, r_recv,
+):
+    dps, xs, zs, chunks = sizes
+    rows, width = grads.shape[0], grads.shape[1] // chunks
+    share = partial.shape[3]
+    f32 = jnp.float32
+    dp_me = lax.axis_index("dp")
+    sp_me = lax.axis_index("sp")
+    x_me = lax.rem(sp_me, xs)
+    z_me = lax.div(sp_me, xs)
+
+    def at_dp(j):
+        return {"dp": dp_me ^ j}
+
+    def at_x(j):
+        return {"sp": z_me * xs + (x_me ^ j)}
+
+    def at_z(j):
+        return {"sp": (z_me ^ j) * xs + x_me}
+
+    def remote(src, dst, send, recv, where):
+        return pltpu.make_async_remote_copy(
+            src_ref=src, dst_ref=dst, send_sem=send, recv_sem=recv,
+            device_id=where, device_id_type=MESH,
+        )
+
+    barrier = pltpu.get_barrier_semaphore()
+    peers = [at_dp(j) for j in range(1, dps)]
+    peers += [at_x(j) for j in range(1, xs)] + [at_z(j) for j in range(1, zs)]
+    for peer in peers:
+        pl.semaphore_signal(barrier, inc=1, device_id=peer, device_id_type=MESH)
+    pl.semaphore_wait(barrier, len(peers))
+
+    def grad_copy(k, j):
+        if j == 1 or j % 2 == 0:
+            return remote(
+                grads.at[:, pl.ds(k * width, width)], held.at[k, j],
+                g_send.at[k, j], g_recv.at[k, j], at_dp(j),
+            )
+        return remote(held.at[k, j - 1], held.at[k, j], g_send.at[k, j], g_recv.at[k, j], at_dp(1))
+
+    def x_copy(k, j):
+        return remote(
+            partial.at[k, x_me ^ j], x_arrived.at[k, j], x_send.at[k, j], x_recv.at[k, j], at_x(j)
+        )
+
+    def z_copy(k, j):
+        return remote(
+            x_sum.at[k, z_me ^ j], z_arrived.at[k, j], z_send.at[k, j], z_recv.at[k, j], at_z(j)
+        )
+
+    def az_send_copy(k, j):
+        block = sums.at[k, x_me, z_me]
+        return remote(block, block, az_send.at[k, j], az_recv.at[k, j], at_z(j))
+
+    def az_recv_copy(k, j):
+        block = sums.at[k, x_me, z_me ^ j]
+        return remote(block, block, az_send.at[k, j], az_recv.at[k, j], at_z(j))
+
+    def ax_send_copy(k, j):
+        block = sums.at[k, x_me]
+        return remote(block, block, ax_send.at[k, j], ax_recv.at[k, j], at_x(j))
+
+    def ax_recv_copy(k, j):
+        block = sums.at[k, x_me ^ j]
+        return remote(block, block, ax_send.at[k, j], ax_recv.at[k, j], at_x(j))
+
+    def result_copy(j):
+        return remote(result.at[j], pieces.at[dp_me], r_send.at[j], r_recv.at[j], at_dp(j))
+
+    def result_recv_copy(j):
+        return remote(result.at[j], pieces.at[dp_me ^ j], r_send.at[j], r_recv.at[j], at_dp(j))
+
+    evens = range(2, dps, 2)
+    odds = range(3, dps, 2)
+    for k in range(chunks):
+        for j in [*evens, 1]:
+            grad_copy(k, j).start()
+    for k in range(chunks):
+        held[k, 0] = grads[:, k * width : (k + 1) * width]
+
+    def first(k):
+        for j in evens:
+            grad_copy(k, j).wait_recv()
+            grad_copy(k, j + 1).start()
+        grad_copy(k, 1).wait_recv()
+        for j in odds:
+            grad_copy(k, j).wait_recv()
+        tokens = held[k].reshape(dps * rows, width)
+        part = jnp.dot(columns[...], tokens, preferred_element_type=f32)
+        partial[k] = part.reshape(xs, zs, share, width).astype(jnp.bfloat16)
+        for j in range(1, xs):
+            x_copy(k, j).start()
+
+    def second(k):
+        total = partial[k, x_me].astype(f32)
+        for j in range(1, xs):
+            x_copy(k, j).wait_recv()
+            total = total + x_arrived[k, j].astype(f32)
+        x_sum[k] = total.astype(jnp.bfloat16)
+        for j in range(1, zs):
+            z_copy(k, j).start()
+
+    def third(k):
+        total = x_sum[k, z_me].astype(f32)
+        for j in range(1, zs):
+            z_copy(k, j).wait_recv()
+            total = total + z_arrived[k, j].astype(f32)
+        sums[k, x_me, z_me] = total.astype(jnp.bfloat16)
+        for j in range(1, zs):
+            az_send_copy(k, j).start()
+
+    def fourth(k):
+        for j in range(1, zs):
+            az_recv_copy(k, j).wait_recv()
+        for j in range(1, xs):
+            ax_send_copy(k, j).start()
+
+    def project():
+        for j in [*range(1, dps), 0]:
+            total = None
+            for k in range(chunks):
+                weight = up_weight if k < chunks // 2 else gate_weight
+                at = k % (chunks // 2) * width
+                term = lax.dot_general(
+                    held[k, j], weight[:, at : at + width],
+                    (((1,), (1,)), ((), ())), preferred_element_type=f32,
+                )
+                total = term if total is None else total + term
+            if j == 0:
+                pieces[dp_me] = total.astype(jnp.bfloat16)
+            else:
+                result[j] = total.astype(jnp.bfloat16)
+                result_copy(j).start()
+
+    for step in range(chunks + 3):
+        for stage, lag in ((first, 0), (second, 1), (third, 2), (fourth, 3)):
+            if 0 <= step - lag < chunks:
+                stage(step - lag)
+        if step == chunks - 1:
+            project()
+    for k in range(chunks):
+        for j in range(1, xs):
+            ax_recv_copy(k, j).wait_recv()
+    for j in range(1, dps):
+        result_recv_copy(j).wait_recv()
+        result_copy(j).wait_send()
+    for k in range(chunks):
+        for j in range(1, dps):
+            grad_copy(k, j).wait_send()
+        for j in range(1, xs):
+            x_copy(k, j).wait_send()
+            ax_send_copy(k, j).wait_send()
+        for j in range(1, zs):
+            z_copy(k, j).wait_send()
+            az_send_copy(k, j).wait_send()
+
+
+def exchange(both_grads, columns, up_weight, gate_weight):
+    dps = lax.axis_size("dp")
+    sps = lax.axis_size("sp")
+    xs = 2 ** ((sps.bit_length() - 1) // 2)
+    zs = sps // xs
+    rows, both_width = both_grads.shape
+    width = both_width // CHUNKS
+    own_columns = columns.shape[0]
+    share = own_columns // sps
+    bf16 = jnp.bfloat16
+    vmem = pl.BlockSpec(memory_space=pltpu.VMEM)
+    dma = pltpu.SemaphoreType.DMA
+    return pl.pallas_call(
+        functools.partial(exchange_kernel, (dps, xs, zs, CHUNKS)),
+        out_shape=(
+            jax.ShapeDtypeStruct((CHUNKS, xs, zs, share, width), bf16),
+            jax.ShapeDtypeStruct((dps, rows, own_columns), bf16),
+        ),
+        in_specs=[vmem] * 4,
+        out_specs=(vmem, vmem),
+        scratch_shapes=[
+            pltpu.VMEM((CHUNKS, dps, rows, width), bf16),
+            pltpu.VMEM((CHUNKS, xs, zs, share, width), bf16),
+            pltpu.VMEM((CHUNKS, xs, zs, share, width), bf16),
+            pltpu.VMEM((CHUNKS, zs, share, width), bf16),
+            pltpu.VMEM((CHUNKS, zs, share, width), bf16),
+            pltpu.VMEM((dps, rows, own_columns), bf16),
+        ]
+        + [dma((CHUNKS, dps))] * 2
+        + [dma((CHUNKS, xs))] * 2
+        + [dma((CHUNKS, zs))] * 4
+        + [dma((CHUNKS, xs))] * 2
+        + [dma((dps,))] * 2,
+        compiler_params=pltpu.CompilerParams(
+            collective_id=0, has_side_effects=True, vmem_limit_bytes=60 * 1024 * 1024
+        ),
+    )(both_grads, columns, up_weight, gate_weight)
 
 
 def on_device(inputs, up_pre, gate_pre, cotangent, norm_gain, up_weight, gate_weight, mix_weight):
@@ -42,7 +241,18 @@
     sp_count = lax.axis_size("sp")
     assert sequences == 1 and own_rows * 2 == SPAN
     groups = gated_width // GROUP_CH
-    input_columns = lax.all_to_all(inputs[0], "dp", split_axis=1, concat_axis=0, tiled=True)
+    dp_count = lax.axis_size("dp")
+    dp_me = lax.axis_index("dp")
+    column_share = model_width // dp_count
+    input_pieces = []
+    for j in range(dp_count):
+        piece = lax.dynamic_slice(
+            inputs[0], (0, (dp_me ^ j) * column_share), (own_rows, column_share)
+        )
+        if j:
+            piece = lax.ppermute(piece, "dp", [(i, i ^ j) for i in range(dp_count)])
+        input_pieces.append(piece)
+    columns = jnp.concatenate(input_pieces, axis=0).T
     up_float = up_pre[0].astype(jnp.float32)
     gate_float = gate_pre[0].astype(jnp.float32)
     grad_float = cotangent[0].astype(jnp.float32)
@@ -84,16 +294,15 @@
     )
     gate_pre_grad = (gated_grad * gelu_slope(gate_float)).astype(jnp.bfloat16)
     both_grads = jnp.concatenate([up_pre_grad, gate_pre_grad], axis=1)
-    all_grads = lax.all_gather(both_grads, "dp", axis=0, tiled=True)
-    weight_part = contract(input_columns, all_grads, 0, 0).astype(jnp.bfloat16)
-    own_part = lax.psum_scatter(weight_part, "sp", scatter_dimension=0, tiled=True)
-    weight_rows = lax.all_gather(own_part, "sp", axis=0, tiled=True).astype(f32)
-    both_weights = jnp.concatenate([up_weight, gate_weight], axis=1)
-    result_part = contract(all_grads, both_weights, 1, 1).astype(jnp.bfloat16)
-    input_grad = lax.all_to_all(result_part, "dp", split_axis=0, concat_axis=1, tiled=True)
-    up_weight_grad = weight_rows[:, :gated_width] * grad_scale
-    gate_weight_grad = weight_rows[:, gated_width:] * grad_scale
-    return (input_grad[None], up_weight_grad, gate_weight_grad)
+    sums, pieces = exchange(both_grads, columns, up_weight, gate_weight)
+    input_grad = pieces.transpose(1, 0, 2).reshape(1, own_rows, model_width)
+    half_chunks = CHUNKS // 2
+
+    def rows_of(part):
+        ordered = part.transpose(1, 2, 3, 0, 4).reshape(column_share, gated_width)
+        return ordered.astype(f32) * grad_scale
+
+    return (input_grad, rows_of(sums[:half_chunks]), rows_of(sums[half_chunks:]))
 
 
 def solution(mesh):

time: 227 us -> 137 us (0.60)
  waiting for transfers between devices: 117 us -> 2.42 us
  Pallas kernels: 0 us -> 78.8 us
  blocking collectives: 40.6 us -> 0 us
  between operations: 13.9 us -> 0.83 us
  matrix products: 17.1 us -> 7.68 us
  local copies, waits for them, and re-layouts: 17 us -> 25.8 us
  other arithmetic: 17.6 us -> 13.8 us
    pallas_call x0 -> x1, Pallas kernels: none -> 78.8 us  [exchange(): pl.pallas_call(functools.partial(exchange_kernel, (dps, xs, zs, CHUNKS)),...]
    reduce_scatter x1 -> x0, waiting for transfers between devices: 68.7 us -> none  [on_device(): lax.psum_scatter(weight_part, 'sp', scatter_dimension=0, tiled=True)]
    all_gather x2 -> x0, waiting for transfers between devices: 43.2 us -> none  [the longest x1 26 us: on_device(): weight_rows = lax.all_gather(own_part, 'sp', axis=0, tiled=True).astype(f32)]
    all_to_all x2 -> x0, blocking collectives: 40.6 us -> none  [the longest x1 23.6 us: on_device(): lax.all_to_all(inputs[0], 'dp', split_axis=1, concat_axis=0, tiled=True)]
    dot_general x2 -> x0, matrix products: 9.41 us -> none  [contract(): lax.dot_general(first_op, second_op, (((first_dim,), (second_dim,)), ((),...]
    dynamic_slice x0 -> x5, local copies, waits for them, and re-layouts: none -> 4.69 us  [on_device(): lax.dynamic_slice(inputs[0], (0, (dp_me ^ j) * column_share), (own_rows,...]
    mul x0 -> x2, local copies, waits for them, and re-layouts: none -> 3.24 us  [rows_of(): return ordered.astype(f32) * grad_scale]
    ppermute x0 -> x3, starting transfers between devices: none -> 3.12 us  [on_device(): piece = lax.ppermute(piece, 'dp', [(i, i ^ j) for i in range(dp_count)])]
  transfers between devices with their start and end apart: 4 -> 4, of which waited for: 4 -> 1; matrix products, arithmetic and copies ran while one was open for 7% -> 10% of each run, Pallas kernels for 0% -> 0%
where the time goes in v2:
time: 137 us; the launch traced here: 134 us
  Pallas kernels  78.8 us (58%)
  local copies, waits for them, and re-layouts  25.8 us (19%)
  other arithmetic  13.8 us (10%)
  matrix products  7.68 us (6%)
  starting transfers between devices  5.11 us (4%)
  waiting for transfers between devices  2.42 us (2%)
    pallas_call x1, Pallas kernels, exchange(): pl.pallas_call(functools.partial(exchange_kernel, (dps, xs, zs, CHUNKS)),...  78.8 us
    unnamed x19, local copies, waits for them, and re-layouts  5.02 us
    dynamic_slice x5, local copies, waits for them, and re-layouts, on_device(): lax.dynamic_slice(inputs[0], (0, (dp_me ^ j) * column_share), (own_rows,...  4.69 us
    mul x2, local copies, waits for them, and re-layouts, rows_of(): return ordered.astype(f32) * grad_scale  3.24 us
    ppermute x3, starting transfers between devices, on_device(): piece = lax.ppermute(piece, 'dp', [(i, i ^ j) for i in range(dp_count)])  3.12 us
    slice x2, local copies, waits for them, and re-layouts, on_device(): cross_block = mix_weight[:, own_rows:, :own_rows]  2.82 us
    dot_general x1, matrix products, on_device(): jnp.einsum('gts,sgc->tgc', own_block, own_in, preferred_element_type=f32)  2.8 us
  transfers between devices with their start and end apart: 4, of which 1 were waited for; matrix products, arithmetic and copies ran while one was open for 10% of the time, Pallas kernels for 0%

profile of v2, /device:TPU:0, one launch (start us, length us, event | category | flops | bytes accessed | tf_op | source)
XLA Modules:
  0.0 134.5 jit_solution(3281522448306304004)
XLA Ops:
  0.7 1.3 constant_dynamic-slice_fusion.3
  2.0 0.8 copy.29
  2.8 3.0 %collective-permute-start.2 = (bf16[256,512]{0,1:T(8,128)(2,1)}, bf16[256,512]{0,1:T(8,128)(2,1)}, u32[]{:S(2)}, u32[]{:S(2)}) collective-permute-start(bf16[256,512]{0,1:T(8,128)(2,1)} %bitcast.15), channel_id=1, source_target_pairs={{0,2},{1,3},{2,0},{3,1},{4,6},{5,7},{6,4},{7,5},{8,10},{9,11},{10,... | collective-permute-start | bytes 786440 | tf_op jit(solution)/shard_map/ppermute | solution.py:253
  5.8 0.8 copy.30
  6.7 0.8 copy.28
  8.3 1.3 fusion.42
  9.6 2.0 %collective-permute-start = (bf16[256,1024]{1,0:T(8,128)(2,1)}, bf16[256,1024]{1,0:T(8,128)(2,1)}, u32[]{:S(2)}, u32[]{:S(2)}) collective-permute-start(bf16[256,1024]{1,0:T(8,128)(2,1)} %fusion.42), channel_id=1, source_target_pairs={{0,4},{4,0},{8,12},{12,8},{16,20},{20,16},{24,28},{28,24},{1,5},{5... | collective-permute-start | bytes 1572872 | tf_op jit(solution)/shard_map/ppermute | solution.py:266
  11.9 1.2 fusion.21
  13.1 1.0 copy.38
  14.1 0.8 copy.27
  14.9 1.3 slice.9
  16.3 1.5 %copy.22 = bf16[8,256,256]{1,2,0:T(8,128)(2,1)} copy(bf16[8,256,256]{2,1,0:T(8,128)(2,1)S(1)} %slice.9) | data formatting | bytes 2097152 | tf_op jit(solution)/shard_map/slice | solution.py:276
  17.8 1.6 %copy.35 = f32[1,256,1024]{1,2,0:T(8,128)S(1)} copy(f32[1,256,1024]{2,1,0:T(8,128)} %fusion.21) | data formatting | bytes 2097152 | tf_op jit(solution)/shard_map/mul | solution.py:23
  19.5 2.3 %maximum_bitcast_fusion.columns = bf16[512,1024]{1,0:T(8,128)(2,1)} fusion(bf16[256,512]{0,1:T(8,128)(2,1)} %collective-permute-done.3, bf16[256,512]{0,1:T(8,128)(2,1)} %collective-permute-done.2, bf16[256,512]{0,1:T(8,128)(2,1)} %collective-permute-done.1, bf16[256,512]{0,1:T(8,128)(2,1)S(1)} %bitcast.140), kind=kLoop, calls=%fused_computation.46 | loop fusion | flops 4194304 | bytes 2097152 | tf_op jit(solution)/shard_map/transpose | solution.py:255
  21.7 2.4 %collective-permute-done = bf16[256,1024]{1,0:T(8,128)(2,1)} collective-permute-done((bf16[256,1024]{1,0:T(8,128)(2,1)}, bf16[256,1024]{1,0:T(8,128)(2,1)}, u32[]{:S(2)}, u32[]{:S(2)}) %collective-permute-start) | collective-permute-done | bytes 524320 | tf_op jit(solution)/shard_map/ppermute | solution.py:266
  24.2 2.0 %copy.36 = bf16[256,1024]{0,1:T(8,128)(2,1)} copy(bf16[256,1024]{1,0:T(8,128)(2,1)} %collective-permute-done) | data formatting | bytes 1048576 | tf_op jit(solution)/shard_map/reshape | solution.py:282
  26.2 2.2 %fusion.35 = f32[8,128,256]{2,1,0:T(8,128)S(1)} fusion(bf16[256,8,128]{0,2,1:T(8,128)(2,1)} %bitcast.138, bf16[8,256,256]{1,2,0:T(8,128)(2,1)} %copy.22, pred[]{:T(512)S(6)} %eq.4, bf16[8,512,512]{2,1,0:T(8,128)(2,1)} %param.15), kind=kOutput, calls=%fused_computation.50 | convolution fusion | flops 134742016 | bytes 3670017 | tf_op jit(solution)/shard_map/gts,sgc->tgc/dot_general | solution.py:282
  28.4 2.8 %fusion.39 = f32[8,128,256]{2,1,0:T(8,128)} fusion(f32[8,128,256]{2,1,0:T(8,128)S(1)} %fusion.35, bf16[8,512,512]{2,1,0:T(8,128)(2,1)} %param.15, s32[]{:T(128)S(6)} %select_n.74, pred[256,256]{1,0:T(8,128)(4,1)S(1)} %broadcast_compare_fusion, f32[256,8,128]{0,2,1:T(8,128)S(1)} %bitcast.128, f32[8,128]{1,0:T(8,128)S(1)} %bitcast.141, ...), kind=kOutput, calls=%fused_computation.62 | convolution fusion | flops 136839168 | bytes 4265989 | tf_op jit(solution)/shard_map/gts,sgc->tgc/dot_general | solution.py:283
  31.2 2.7 %fusion.34 = (f32[256]{0:T(256)S(1)}, f32[8,128,256]{2,1,0:T(8,128)}) fusion(f32[256,8,128]{0,2,1:T(8,128)S(1)} %bitcast.129, f32[8,128]{1,0:T(8,128)S(1)} %bitcast.142, f32[256]{0:T(256)S(1)} %add_rsqrt_fusion, f32[256]{0:T(256)S(1)} %broadcast_multiply_fusion.2, f32[8,128,256]{2,1,0:T(8,128)S(1)} %fusion.35, pred[]{:T(512)S(6)} %eq.4, ...), kind=kOutput, calls=%fused_computation.48 | convolution fusion | flops 137101056 | bytes 4791301 | tf_op jit(solution)/shard_map/gts,tgc->sgc/dot_general | solution.py:284
  33.9 2.6 %copy.37 = f32[256,1024]{1,0:T(8,128)} copy(f32[256,1024]{0,1:T(8,128)} %bitcast.133) | data formatting | bytes 2097152 | tf_op jit(solution)/shard_map/convert_element_type | solution.py:288
  36.5 2.7 %fusion.12 = bf16[256,1024]{1,0:T(8,128)(2,1)} fusion(f32[256,1024]{1,0:T(8,128)} %copy.37, bf16[1,256,1024]{2,1,0:T(8,128)(2,1)} %param.11, bf16[1,256,1024]{2,1,0:T(8,128)(2,1)S(1)} %copy-done.2), kind=kLoop, calls=%fused_computation.23 | loop fusion | flops 3407872 | bytes 2621440 | tf_op jit(solution)/shard_map/convert_element_type | solution.py:288
  39.4 1.3 copy.39
  40.7 2.0 %fusion.20 = bf16[256,1024]{1,0:T(8,128)(2,1)S(1)} fusion(bf16[1,256,1024]{2,1,0:T(8,128)(2,1)S(1)} %copy-done, f32[256,1024]{1,0:T(8,128)S(1)} %get-tuple-element.11, f32[256,1024]{1,0:T(8,128)} %copy.39, f32[256]{0:T(256)S(1)} %get-tuple-element.20, f32[256]{0:T(256)S(1)} %get-tuple-element.21, f32[1024]{0:T(1024)S(1)} %copy-done.7, ...), kind=kLoop, calls=%fused_computation.31 | loop fusion | flops 4718592 | bytes 3153920 | tf_op jit(solution)/shard_map/convert_element_type | solution.py:295
  42.7 1.1 pad_maximum_fusion.grads
  43.8 78.8 %shard_map.103 = (bf16[4,2,4,64,512]{4,3,2,1,0:T(8,128)(2,1)}, bf16[4,256,512]{2,1,0:T(8,128)(2,1)}) custom-call(bf16[256,2048]{1,0:T(8,128)(2,1)} %pad_maximum_fusion.grads, bf16[512,1024]{1,0:T(8,128)(2,1)} %maximum_bitcast_fusion.columns, bf16[512,1024]{1,0:T(8,128)(2,1)} %up_weight.1, bf16[512,1024]{1,0:T(8,128)(2,1)} %gate_weight.1), custom_call_target="tpu_custom_call" | custom-call | tf_op jit(solution)/shard_map/pallas_call | solution.py:211
  122.6 1.5 %copy.31 = bf16[256,4,512]{0,2,1:T(8,128)(2,1)S(1)} copy(bf16[256,4,512]{2,0,1:T(8,128)(2,1)} %bitcast.139) | data formatting | bytes 2097152 | tf_op jit(solution)/shard_map/transpose | solution.py:298
  124.1 1.4 %copy.34 = bf16[1,256,2048]{2,1,0:T(8,128)(2,1)} copy(bf16[1,256,2048]{1,2,0:T(8,128)(2,1)S(1)} %bitcast.134) | data formatting | bytes 2097152
  125.5 2.1 %multiply_bitcast_fusion = (f32[2,4,64,2,512]{4,2,1,0,3:T(8,128)S(1)}, f32[2,4,64,2,512]{4,2,1,0,3:T(8,128)S(1)}) fusion(bf16[4,2,4,64,512]{4,3,2,1,0:T(8,128)(2,1)} %get-tuple-element.6), kind=kLoop, calls=%fused_computation | loop fusion | flops 2097152 | bytes 6291456 | tf_op jit(solution)/shard_map/mul | solution.py:303
  127.6 1.6 %copy.33 = f32[2,4,64,2,512]{4,3,2,1,0:T(2,128)S(1)} copy(f32[2,4,64,2,512]{4,2,1,0,3:T(8,128)S(1)} %get-tuple-element.12) | data formatting | bytes 4194304 | tf_op jit(solution)/shard_map/mul | solution.py:303
  129.3 1.8 %copy.41 = f32[64,8,2,512]{3,1,2,0:T(8,128)} copy(f32[64,8,2,512]{3,2,1,0:T(2,128)S(1)} %bitcast.131) | data formatting | bytes 4194304
  131.1 1.6 %copy.32 = f32[2,4,64,2,512]{4,3,2,1,0:T(2,128)S(1)} copy(f32[2,4,64,2,512]{4,2,1,0,3:T(8,128)S(1)} %get-tuple-element.13) | data formatting | bytes 4194304 | tf_op jit(solution)/shard_map/mul | solution.py:303
  132.7 1.8 %copy.40 = f32[64,8,2,512]{3,1,2,0:T(8,128)} copy(f32[64,8,2,512]{3,2,1,0:T(2,128)S(1)} %bitcast.132) | data formatting | bytes 4194304
  (30 shorter events, 1.4 us)
Async XLA Ops:
  0.6 7.0 %copy-start = (bf16[1,256,1024]{2,1,0:T(8,128)(2,1)S(1)}, bf16[1,256,1024]{2,1,0:T(8,128)(2,1)}, u32[]{:S(2)}) copy-start(bf16[1,256,1024]{2,1,0:T(8,128)(2,1)} %param.10) | copy-start | bytes 1572868
  2.8 16.6 %collective-permute-start.2 = (bf16[256,512]{0,1:T(8,128)(2,1)}, bf16[256,512]{0,1:T(8,128)(2,1)}, u32[]{:S(2)}, u32[]{:S(2)}) collective-permute-start(bf16[256,512]{0,1:T(8,128)(2,1)} %bitcast.15), channel_id=1, source_target_pairs={{0,2},{1,3},{2,0},{3,1},{4,6},{5,7},{6,4},{7,5},{8,10},{9,11},{10,... | collective-permute-start | bytes 786440 | tf_op jit(solution)/shard_map/ppermute | solution.py:253
  5.8 2.4 %copy-start.2 = (bf16[1,256,1024]{2,1,0:T(8,128)(2,1)S(1)}, bf16[1,256,1024]{2,1,0:T(8,128)(2,1)}, u32[]{:S(2)}) copy-start(bf16[1,256,1024]{2,1,0:T(8,128)(2,1)} %param.9) | copy-start | bytes 1572868
  5.8 2.5 %copy-start.3 = (bf16[1,256,1024]{2,1,0:T(8,128)(2,1)S(1)}, bf16[1,256,1024]{2,1,0:T(8,128)(2,1)}, u32[]{:S(2)}) copy-start(bf16[1,256,1024]{2,1,0:T(8,128)(2,1)} %param.11) | copy-start | bytes 1572868
  5.8 2.5 %copy-start.7 = (f32[1024]{0:T(1024)S(1)}, f32[1024]{0:T(1024)}, u32[]{:S(2)}) copy-start(f32[1024]{0:T(1024)} %param.12) | copy-start | bytes 12292
  6.7 12.8 %collective-permute-start.3 = (bf16[256,512]{0,1:T(8,128)(2,1)}, bf16[256,512]{0,1:T(8,128)(2,1)}, u32[]{:S(2)}, u32[]{:S(2)}) collective-permute-start(bf16[256,512]{0,1:T(8,128)(2,1)} %bitcast.16), channel_id=1, source_target_pairs={{0,3},{1,2},{2,1},{3,0},{4,7},{5,6},{6,5},{7,4},{8,11},{9,10},{10,... | collective-permute-start | bytes 786440 | tf_op jit(solution)/shard_map/ppermute | solution.py:253
  7.5 12.0 %collective-permute-start.1 = (bf16[256,512]{0,1:T(8,128)(2,1)}, bf16[256,512]{0,1:T(8,128)(2,1)}, u32[]{:S(2)}, u32[]{:S(2)}) collective-permute-start(bf16[256,512]{0,1:T(8,128)(2,1)} %bitcast.14), channel_id=1, source_target_pairs={{0,1},{1,0},{2,3},{3,2},{4,5},{5,4},{6,7},{7,6},{8,9},{9,8},{10,11... | collective-permute-start | bytes 786440 | tf_op jit(solution)/shard_map/ppermute | solution.py:253
  9.6 14.5 %collective-permute-start = (bf16[256,1024]{1,0:T(8,128)(2,1)}, bf16[256,1024]{1,0:T(8,128)(2,1)}, u32[]{:S(2)}, u32[]{:S(2)}) collective-permute-start(bf16[256,1024]{1,0:T(8,128)(2,1)} %fusion.42), channel_id=1, source_target_pairs={{0,4},{4,0},{8,12},{12,8},{16,20},{20,16},{24,28},{28,24},{1,5},{5... | collective-permute-start | bytes 1572872 | tf_op jit(solution)/shard_map/ppermute | solution.py:266
  16.3 3.2 %copy-start.6 = (bf16[1,256,512]{1,2,0:T(8,128)(2,1)S(1)}, bf16[1,256,512]{1,2,0:T(8,128)(2,1)}, u32[]{:S(2)}) copy-start(bf16[1,256,512]{1,2,0:T(8,128)(2,1)} %copy.27) | copy-start | bytes 786436
  28.4 2.8 %copy-start.4 = (bf16[1,256,1024]{1,2,0:T(8,128)(2,1)S(1)}, bf16[1,256,1024]{1,2,0:T(8,128)(2,1)}, u32[]{:S(2)}) copy-start(bf16[1,256,1024]{1,2,0:T(8,128)(2,1)} %copy.38) | copy-start | bytes 1572868
  33.9 5.3 %copy-start.1 = (f32[8,128,256]{2,1,0:T(8,128)S(1)}, f32[8,128,256]{2,1,0:T(8,128)}, u32[]{:S(2)}) copy-start(f32[8,128,256]{2,1,0:T(8,128)} %get-tuple-element.19) | copy-start | bytes 3145732
  40.7 2.0 %copy-start.5 = (bf16[256,1024]{1,0:T(8,128)(2,1)S(1)}, bf16[256,1024]{1,0:T(8,128)(2,1)}, u32[]{:S(2)}) copy-start(bf16[256,1024]{1,0:T(8,128)(2,1)} %fusion.12) | copy-start | bytes 1572868

commit v3 on v2

v3 whole, which is shorter than its diff:
```python
import functools
import math

import jax
import jax.numpy as jnp
from jax import lax
from jax.experimental import pallas as pl
from jax.experimental.pallas import tpu as pltpu
from jax.sharding import PartitionSpec as P

GROUP_CH = 128
SPAN = 512
SEG = 64


norm_eps = 1e-05
grad_scale = 1.0 / 256.0
root_half = 1.0 / math.sqrt(2.0)
root_twopi = 1.0 / math.sqrt(2.0 * math.pi)


CHUNKS = 8
BAND = 16
MESH = pl.DeviceIdType.MESH


def exchange_kernel(
    sizes, inputs, up_pre, gate_pre, cotangent, gain, up_hbm, gate_hbm, mix_hbm, sums, pieces,
    up_weight, gate_weight, mix, own, other, normed_at, inverse_at, up_slope, gate_slope,
    spatial, back, col_arrived, columns,
    held, partial, x_arrived, x_sum, z_arrived, result,
    load, c_send, c_recv, p_send, p_recv,
    g_send, g_recv, x_send, x_recv, z_send, z_recv,
    az_send, az_recv, ax_send, ax_recv, r_send, r_recv,
):
    dps, xs, zs, chunks = sizes
    rows, gated = own.shape[1:]
    width = 2 * gated // chunks
    column_share = columns.shape[0]
    share = partial.shape[3]
    f32 = jnp.float32
    dp_me = lax.axis_index("dp")
    sp_me = lax.axis_index("sp")
    x_me = lax.rem(sp_me, xs)
    z_me = lax.div(sp_me, xs)

    def at_dp(j):
        return {"dp": dp_me ^ j}

    def at_x(j):
        return {"sp": z_me * xs + (x_me ^ j)}

    def at_z(j):
        return {"sp": (z_me ^ j) * xs + x_me}

    def remote(src, dst, send, recv, where):
        return pltpu.make_async_remote_copy(
            src_ref=src, dst_ref=dst, send_sem=send, recv_sem=recv,
            device_id=where, device_id_type=MESH,
        )

    loads = [
        pltpu.make_async_copy(mix_hbm, mix, load.at[0]),
        pltpu.make_async_copy(up_hbm, up_weight, load.at[1]),
        pltpu.make_async_copy(gate_hbm, gate_weight, load.at[2]),
    ]
    for copy in loads:
        copy.start()
    barrier = pltpu.get_barrier_semaphore()
    peers = [at_dp(j) for j in range(1, dps)]
    peers += [at_x(j) for j in range(1, xs)] + [at_z(j) for j in range(1, zs)]
    for peer in peers:
        pl.semaphore_signal(barrier, inc=1, device_id=peer, device_id_type=MESH)
    pl.semaphore_wait(barrier, len(peers))

    def grad_copy(k, j):
        if j == 1 or j % 2 == 0:
            return remote(
                held.at[k, 0], held.at[k, j],
                g_send.at[k, j], g_recv.at[k, j], at_dp(j),
            )
        return remote(held.at[k, j - 1], held.at[k, j], g_send.at[k, j], g_recv.at[k, j], at_dp(1))

    def x_copy(k, j):
        return remote(
            partial.at[k, x_me ^ j], x_arrived.at[k, j], x_send.at[k, j], x_recv.at[k, j], at_x(j)
        )

    def z_copy(k, j):
        return remote(
            x_sum.at[k, z_me ^ j], z_arrived.at[k, j], z_send.at[k, j], z_recv.at[k, j], at_z(j)
        )

    def az_send_copy(k, j):
        block = sums.at[x_me, z_me, :, pl.ds(k * width, width)]
        return remote(block, block, az_send.at[k, j], az_recv.at[k, j], at_z(j))

    def az_recv_copy(k, j):
        block = sums.at[x_me, z_me ^ j, :, pl.ds(k * width, width)]
        return remote(block, block, az_send.at[k, j], az_recv.at[k, j], at_z(j))

    def ax_send_copy(k, j):
        block = sums.at[x_me, :, :, pl.ds(k * width, width)]
        return remote(block, block, ax_send.at[k, j], ax_recv.at[k, j], at_x(j))

    def ax_recv_copy(k, j):
        block = sums.at[x_me ^ j, :, :, pl.ds(k * width, width)]
        return remote(block, block, ax_send.at[k, j], ax_recv.at[k, j], at_x(j))

    def columns_of(who):
        return pl.ds(pl.multiple_of(who * column_share, column_share), column_share)

    def column_copy(j):
        return remote(
            inputs.at[:, columns_of(dp_me ^ j)], col_arrived.at[j],
            c_send.at[j], c_recv.at[j], at_dp(j),
        )

    half = lax.rem(sp_me, 2)
    part_rows = rows // 2

    def pair_copy(b):
        span = pl.ds(b * part_rows, part_rows)
        return remote(own.at[half, span], other.at[span], p_send.at[b], p_recv.at[b], at_x(1))

    def result_copy(j):
        return remote(result.at[j], pieces.at[:, columns_of(dp_me)], r_send.at[j], r_recv.at[j], at_dp(j))

    def result_recv_copy(j):
        return remote(result.at[j], pieces.at[:, columns_of(dp_me ^ j)], r_send.at[j], r_recv.at[j], at_dp(j))

    evens = range(2, dps, 2)
    odds = range(3, dps, 2)
    for j in range(1, dps):
        column_copy(j).start()

    def slopes(band):
        at = pl.ds(pl.multiple_of(band * BAND, BAND), BAND)
        gate = gate_pre[at, :].astype(f32)
        cdf = 0.5 * (1.0 + lax.erf(gate * root_half))
        gate_slope[at, :] = cdf + gate * jnp.exp(-0.5 * gate * gate) * root_twopi
        act = gate * cdf
        centered = act - jnp.mean(act, axis=-1, keepdims=True)
        inverse = lax.rsqrt(jnp.mean(centered * centered, axis=-1, keepdims=True) + norm_eps)
        normed = centered * inverse
        normed_at[at, :] = normed
        inverse_at[at, :] = jnp.broadcast_to(inverse, (BAND, 128))
        own[0, at, :] = (normed * gain[...]).astype(jnp.bfloat16)
        up = up_pre[at, :].astype(f32)
        grad = cotangent[at, :].astype(f32)
        cdf = 0.5 * (1.0 + lax.erf(up * root_half))
        up_slope[at, :] = grad * (cdf + up * jnp.exp(-0.5 * up * up) * root_twopi)
        own[1, at, :] = (grad * (up * cdf)).astype(jnp.bfloat16)

    bands = part_rows // BAND
    for b in range(2):
        pl.loop(b * bands, (b + 1) * bands)(slopes)
        pair_copy(b).start()

    loads[0].wait()
    own_rows = pl.ds(pl.multiple_of(half * rows, rows), rows)
    row_segment = lax.broadcasted_iota(jnp.int32, (rows, rows), 0) // SEG
    column_segment = lax.broadcasted_iota(jnp.int32, (rows, rows), 1) // SEG
    seen = column_segment <= row_segment
    groups = mix.shape[0]

    def group_dot(weight, value, dim):
        return lax.dot_general(
            weight, value, (((dim,), (0,)), ((), ())), preferred_element_type=f32
        )

    for g in range(groups):
        lanes = slice(g * GROUP_CH, (g + 1) * GROUP_CH)
        block = mix[g, own_rows, own_rows]
        block = jnp.where(seen, block, jnp.zeros_like(block))
        spatial[:, lanes] = group_dot(block, own[0, :, lanes], 1)
        back[:, lanes] = group_dot(block, own[1, :, lanes], 0)
    for b in range(2):
        pair_copy(b).wait_recv()

    @pl.when(half == 1)
    def _():
        for g in range(groups):
            lanes = slice(g * GROUP_CH, (g + 1) * GROUP_CH)
            spatial[:, lanes] += group_dot(mix[g, rows:, :rows], other[:, lanes], 1)

    @pl.when(half == 0)
    def _():
        for g in range(groups):
            lanes = slice(g * GROUP_CH, (g + 1) * GROUP_CH)
            back[:, lanes] += group_dot(mix[g, rows:, :rows], other[:, lanes], 0)

    def up_band(band):
        at = pl.ds(pl.multiple_of(band * BAND, BAND), BAND)
        mixed = spatial[at, :].astype(jnp.bfloat16).astype(f32)
        grad = (mixed * up_slope[at, :]).astype(jnp.bfloat16)
        for k in range(chunks // 2):
            held[k, 0, at, :] = grad[:, k * width : (k + 1) * width]

    def gate_band(band):
        at = pl.ds(pl.multiple_of(band * BAND, BAND), BAND)
        scaled = back[at, :].astype(jnp.bfloat16).astype(f32) * gain[...]
        normed = normed_at[at, :]
        grad = inverse_at[at, 0:1] * (
            scaled
            - jnp.mean(scaled, axis=-1, keepdims=True)
            - normed * jnp.mean(scaled * normed, axis=-1, keepdims=True)
        )
        grad = (grad * gate_slope[at, :]).astype(jnp.bfloat16)
        for k in range(chunks // 2):
            held[chunks // 2 + k, 0, at, :] = grad[:, k * width : (k + 1) * width]

    pl.loop(0, rows // BAND)(up_band)
    for k in range(chunks // 2):
        for j in [*evens, 1]:
            grad_copy(k, j).start()
    pl.loop(0, rows // BAND)(gate_band)
    for k in range(chunks // 2, chunks):
        for j in [*evens, 1]:
            grad_copy(k, j).start()
    columns[:, :rows] = inputs[:, columns_of(dp_me)].T
    for j in range(1, dps):
        column_copy(j).wait_recv()
        columns[:, j * rows : (j + 1) * rows] = col_arrived[j].T

    def first(k):
        for j in evens:
            grad_copy(k, j).wait_recv()
            grad_copy(k, j + 1).start()
        grad_copy(k, 1).wait_recv()
        for j in odds:
            grad_copy(k, j).wait_recv()
        tokens = held[k].reshape(dps * rows, width)
        part = jnp.dot(columns[...], tokens, preferred_element_type=f32)
        partial[k] = part.reshape(xs, zs, share, width).astype(jnp.bfloat16)
        for j in range(1, xs):
            x_copy(k, j).start()

    def second(k):
        total = partial[k, x_me].astype(f32)
        for j in range(1, xs):
            x_copy(k, j).wait_recv()
            total = total + x_arrived[k, j].astype(f32)
        x_sum[k] = total.astype(jnp.bfloat16)
        for j in range(1, zs):
            z_copy(k, j).start()

    def third(k):
        total = x_sum[k, z_me].astype(f32)
        for j in range(1, zs):
            z_copy(k, j).wait_recv()
            total = total + z_arrived[k, j].astype(f32)
        sums[x_me, z_me, :, k * width : (k + 1) * width] = total.astype(jnp.bfloat16)
        for j in range(1, zs):
            az_send_copy(k, j).start()

    def fourth(k):
        for j in range(1, zs):
            az_recv_copy(k, j).wait_recv()
        for j in range(1, xs):
            ax_send_copy(k, j).start()

    def project():
        loads[1].wait()
        loads[2].wait()
        for j in [*range(1, dps), 0]:
            total = None
            for k in range(chunks):
                weight = up_weight if k < chunks // 2 else gate_weight
                at = k % (chunks // 2) * width
                term = lax.dot_general(
                    held[k, j], weight[:, at : at + width],
                    (((1,), (1,)), ((), ())), preferred_element_type=f32,
                )
                total = term if total is None else total + term
            if j == 0:
                pieces[:, columns_of(dp_me)] = total.astype(jnp.bfloat16)
            else:
                result[j] = total.astype(jnp.bfloat16)
                result_copy(j).start()

    for step in range(chunks + 3):
        for stage, lag in ((first, 0), (second, 1), (third, 2), (fourth, 3)):
            if 0 <= step - lag < chunks:
                stage(step - lag)
        if step == chunks - 1:
            project()
    for k in range(chunks):
        for j in range(1, xs):
            ax_recv_copy(k, j).wait_recv()
    for b in range(2):
        pair_copy(b).wait_send()
    for j in range(1, dps):
        column_copy(j).wait_send()
        result_recv_copy(j).wait_recv()
        result_copy(j).wait_send()
    for k in range(chunks):
        for j in range(1, dps):
            grad_copy(k, j).wait_send()
        for j in range(1, xs):
            x_copy(k, j).wait_send()
            ax_send_copy(k, j).wait_send()
        for j in range(1, zs):
            z_copy(k, j).wait_send()
            az_send_copy(k, j).wait_send()


def on_device(inputs, up_pre, gate_pre, cotangent, norm_gain, up_weight, gate_weight, mix_weight):
    sequences, rows, gated = cotangent.shape
    model_width = inputs.shape[2]
    assert sequences == 1 and rows * 2 == SPAN
    dps = lax.axis_size("dp")
    sps = lax.axis_size("sp")
    xs = 2 ** ((sps.bit_length() - 1) // 2)
    zs = sps // xs
    width = 2 * gated // CHUNKS
    own_columns = model_width // dps
    share = own_columns // sps
    bf16 = jnp.bfloat16
    f32 = jnp.float32
    vmem = pl.BlockSpec(memory_space=pltpu.VMEM)
    hbm = pl.BlockSpec(memory_space=pl.ANY)
    dma = pltpu.SemaphoreType.DMA
    flat = (rows, gated)
    sums, input_grad = pl.pallas_call(
        functools.partial(exchange_kernel, (dps, xs, zs, CHUNKS)),
        out_shape=(
            jax.ShapeDtypeStruct((xs, zs, share, 2 * gated), bf16),
            jax.ShapeDtypeStruct((rows, model_width), bf16),
        ),
        in_specs=[vmem] * 5 + [hbm] * 3,
        out_specs=(vmem, vmem),
        scratch_shapes=[
            pltpu.VMEM(up_weight.shape, bf16),
            pltpu.VMEM(gate_weight.shape, bf16),
            pltpu.VMEM(mix_weight.shape, bf16),
            pltpu.VMEM((2, *flat), bf16),
            pltpu.VMEM(flat, bf16),
            pltpu.VMEM(flat, f32),
            pltpu.VMEM((rows, 128), f32),
            pltpu.VMEM(flat, f32),
            pltpu.VMEM(flat, f32),
            pltpu.VMEM(flat, f32),
            pltpu.VMEM(flat, f32),
            pltpu.VMEM((dps, rows, own_columns), bf16),
            pltpu.VMEM((own_columns, dps * rows), bf16),
            pltpu.VMEM((CHUNKS, dps, rows, width), bf16),
            pltpu.VMEM((CHUNKS, xs, zs, share, width), bf16),
            pltpu.VMEM((CHUNKS, xs, zs, share, width), bf16),
            pltpu.VMEM((CHUNKS, zs, share, width), bf16),
            pltpu.VMEM((CHUNKS, zs, share, width), bf16),
            pltpu.VMEM((dps, rows, own_columns), bf16),
        ]
        + [dma((3,))]
        + [dma((dps,))] * 2
        + [dma((2,))] * 2
        + [dma((CHUNKS, dps))] * 2
        + [dma((CHUNKS, xs))] * 2
        + [dma((CHUNKS, zs))] * 4
        + [dma((CHUNKS, xs))] * 2
        + [dma((dps,))] * 2,
        compiler_params=pltpu.CompilerParams(
            collective_id=0, has_side_effects=True, vmem_limit_bytes=60 * 1024 * 1024
        ),
    )(
        inputs[0], up_pre[0], gate_pre[0], cotangent[0], norm_gain[None],
        up_weight, gate_weight, mix_weight,
    )
    weight_rows = sums.reshape(own_columns, 2 * gated).astype(f32) * grad_scale
    return (input_grad[None], weight_rows[:, :gated], weight_rows[:, gated:])


def solution(mesh):
    return jax.shard_map(
        on_device,
        mesh=mesh,
        in_specs=(
            P("dp", "sp", None),
            P("dp", "sp", None),
            P("dp", "sp", None),
            P("dp", "sp", None),
            P(),
            P("dp", None),
            P("dp", None),
            P(),
        ),
        out_specs=(P("dp", "sp", None), P("dp", None), P("dp", None)),
        check_vma=False,
    )
```

time: 137 us -> 97 us (0.71); the launches traced: 134 us -> 96.8 us
  local copies, waits for them, and re-layouts: 25.8 us -> 3.29 us
  Pallas kernels: 78.8 us -> 90.8 us
  other arithmetic: 13.8 us -> 2.13 us
  matrix products: 7.68 us -> 0 us
  starting transfers between devices: 5.11 us -> 0 us
  waiting for transfers between devices: 2.42 us -> 0 us
    pallas_call x1, Pallas kernels: 78.8 us -> 90.8 us  [on_device(): pl.pallas_call(functools.partial(exchange_kernel, (dps, xs, zs, CHUNKS)),...]
    dot_general x3 -> x0, matrix products: 7.68 us -> none  [the longest x1 2.8 us: on_device(): jnp.einsum('gts,sgc->tgc', own_block, own_in, preferred_element_type=f32)]
    ppermute x4 -> x0, starting transfers between devices: 5.11 us -> none  [the longest x3 3.12 us: on_device(): piece = lax.ppermute(piece, 'dp', [(i, i ^ j) for i in range(dp_count)])]
    convert_element_type x3 -> x0, other arithmetic: 4.95 us -> none  [the longest x1 2.68 us: on_device(): (grad_float * spatial.astype(f32) * gelu_slope(up_float)).astype(jnp.bflo...]
    convert_element_type x3 -> x0, local copies, waits for them, and re-layouts: 4.93 us -> none  [the longest x1 2.62 us: on_device(): spatial.astype(f32)]
    mul x3 -> x0, local copies, waits for them, and re-layouts: 4.79 us -> none  [the longest x2 3.24 us: rows_of(): return ordered.astype(f32) * grad_scale]
    dynamic_slice x5 -> x0, local copies, waits for them, and re-layouts: 4.69 us -> none  [on_device(): lax.dynamic_slice(inputs[0], (0, (dp_me ^ j) * column_share), (own_rows,...]
    unnamed x19 -> x3, local copies, waits for them, and re-layouts: 5.02 us -> 0.97 us
  transfers between devices with their start and end apart: 4 -> 0, of which waited for: 1 -> 0; matrix products, arithmetic and copies ran while one was open for 10% -> 0% of each run, Pallas kernels for 0% -> 0%
where the time goes in v3:
time: 97 us; the launch traced here: 96.8 us
  Pallas kernels  90.8 us (94%)
  local copies, waits for them, and re-layouts  3.29 us (3%)
  other arithmetic  2.13 us (2%)
    pallas_call x1, Pallas kernels, on_device(): pl.pallas_call(functools.partial(exchange_kernel, (dps, xs, zs, CHUNKS)),...  90.8 us
    slice x1, local copies, waits for them, and re-layouts, on_device(): return (input_grad[None], weight_rows[:, :gated], weight_rows[:, gated:])  2.32 us
    mul x1, other arithmetic, on_device(): weight_rows = sums.reshape(own_columns, 2 * gated).astype(f32) * grad_scale  2.13 us

profile of v3, /device:TPU:0, one launch (start us, length us, event | category | flops | bytes accessed | tf_op | source)
XLA Modules:
  0.0 96.8 jit_solution(7281067773443876507)
XLA Ops:
  0.6 90.8 %shard_map.103 = (bf16[2,4,64,2048]{3,2,1,0:T(8,128)(2,1)}, bf16[256,2048]{1,0:T(8,128)(2,1)}) custom-call(bf16[256,2048]{1,0:T(8,128)(2,1)} %bitcast.9, bf16[256,1024]{1,0:T(8,128)(2,1)} %bitcast.10, bf16[256,1024]{1,0:T(8,128)(2,1)} %bitcast.11, bf16[256,1024]{1,0:T(8,128)(2,1)} %bitcast.12, f32[1,1024]{1,0:T(1,128)} %bitcast.13, ...), custom_call_target="tpu_custom_call" | custom-call | tf_op jit(solution)/shard_map/pallas_call | solution.py:325
  91.4 2.1 %convert_multiply_fusion = f32[2,4,64,2048]{3,2,1,0:T(8,128)S(1)} fusion(bf16[2,4,64,2048]{3,2,1,0:T(8,128)(2,1)} %get-tuple-element.6), kind=kLoop, calls=%fused_computation | loop fusion | flops 2097152 | bytes 6291456 | tf_op jit(solution)/shard_map/mul | solution.py:369
  93.5 0.0 copy-start
  93.6 2.3 %fusion = (f32[512,1024]{1,0:T(8,128)}, f32[512,1024]{1,0:T(8,128)}) fusion(f32[512,2048]{1,0:T(8,128)S(1)} %bitcast.7), kind=kLoop, calls=%fused_computation.1 | loop fusion | bytes 8388608 | tf_op jit(solution)/shard_map/slice | solution.py:370
  95.9 0.0 copy-done
  95.9 1.0 %copy.12 = bf16[1,256,2048]{2,1,0:T(8,128)(2,1)} copy(bf16[1,256,2048]{2,1,0:T(8,128)(2,1)S(1)} %bitcast.8) | data formatting | bytes 2097152
Async XLA Ops:
  93.5 2.3 %copy-start = (bf16[256,2048]{1,0:T(8,128)(2,1)S(1)}, bf16[256,2048]{1,0:T(8,128)(2,1)}, u32[]{:S(2)}) copy-start(bf16[256,2048]{1,0:T(8,128)(2,1)} %get-tuple-element.5) | copy-start | bytes 3145732

commit v4 on v3

--- a/solution.py
+++ b/solution.py
@@ -44,6 +44,12 @@
     x_me = lax.rem(sp_me, xs)
     z_me = lax.div(sp_me, xs)
 
+    def lanes_of(k):
+        return pl.ds(pl.multiple_of(k * width, width), width)
+
+    def order(k):
+        return lax.rem(k + lax.rem(sp_me, 2) * (chunks // 2), chunks)
+
     def at_dp(j):
         return {"dp": dp_me ^ j}
 
@@ -92,19 +98,19 @@
         )
 
     def az_send_copy(k, j):
-        block = sums.at[x_me, z_me, :, pl.ds(k * width, width)]
+        block = sums.at[x_me, z_me, :, lanes_of(k)]
         return remote(block, block, az_send.at[k, j], az_recv.at[k, j], at_z(j))
 
     def az_recv_copy(k, j):
-        block = sums.at[x_me, z_me ^ j, :, pl.ds(k * width, width)]
+        block = sums.at[x_me, z_me ^ j, :, lanes_of(k)]
         return remote(block, block, az_send.at[k, j], az_recv.at[k, j], at_z(j))
 
     def ax_send_copy(k, j):
-        block = sums.at[x_me, :, :, pl.ds(k * width, width)]
+        block = sums.at[x_me, :, :, lanes_of(k)]
         return remote(block, block, ax_send.at[k, j], ax_recv.at[k, j], at_x(j))
 
     def ax_recv_copy(k, j):
-        block = sums.at[x_me ^ j, :, :, pl.ds(k * width, width)]
+        block = sums.at[x_me ^ j, :, :, lanes_of(k)]
         return remote(block, block, ax_send.at[k, j], ax_recv.at[k, j], at_x(j))
 
     def columns_of(who):
@@ -175,20 +181,10 @@
         block = jnp.where(seen, block, jnp.zeros_like(block))
         spatial[:, lanes] = group_dot(block, own[0, :, lanes], 1)
         back[:, lanes] = group_dot(block, own[1, :, lanes], 0)
-    for b in range(2):
-        pair_copy(b).wait_recv()
-
-    @pl.when(half == 1)
-    def _():
-        for g in range(groups):
-            lanes = slice(g * GROUP_CH, (g + 1) * GROUP_CH)
-            spatial[:, lanes] += group_dot(mix[g, rows:, :rows], other[:, lanes], 1)
-
-    @pl.when(half == 0)
-    def _():
-        for g in range(groups):
-            lanes = slice(g * GROUP_CH, (g + 1) * GROUP_CH)
-            back[:, lanes] += group_dot(mix[g, rows:, :rows], other[:, lanes], 0)
+    def send_grads(ks):
+        for k in ks:
+            for j in [*evens, 1]:
+                grad_copy(order(k), j).start()
 
     def up_band(band):
         at = pl.ds(pl.multiple_of(band * BAND, BAND), BAND)
@@ -210,14 +206,33 @@
         for k in range(chunks // 2):
             held[chunks // 2 + k, 0, at, :] = grad[:, k * width : (k + 1) * width]
 
-    pl.loop(0, rows // BAND)(up_band)
-    for k in range(chunks // 2):
-        for j in [*evens, 1]:
-            grad_copy(k, j).start()
-    pl.loop(0, rows // BAND)(gate_band)
-    for k in range(chunks // 2, chunks):
-        for j in [*evens, 1]:
-            grad_copy(k, j).start()
+    @pl.when(half == 0)
+    def _():
+        pl.loop(0, rows // BAND)(up_band)
+
+    @pl.when(half == 1)
+    def _():
+        pl.loop(0, rows // BAND)(gate_band)
+
+    send_grads(range(chunks // 2))
+    for b in range(2):
+        pair_copy(b).wait_recv()
+
+    @pl.when(half == 1)
+    def _():
+        for g in range(groups):
+            lanes = slice(g * GROUP_CH, (g + 1) * GROUP_CH)
+            spatial[:, lanes] += group_dot(mix[g, rows:, :rows], other[:, lanes], 1)
+        pl.loop(0, rows // BAND)(up_band)
+
+    @pl.when(half == 0)
+    def _():
+        for g in range(groups):
+            lanes = slice(g * GROUP_CH, (g + 1) * GROUP_CH)
+            back[:, lanes] += group_dot(mix[g, rows:, :rows], other[:, lanes], 0)
+        pl.loop(0, rows // BAND)(gate_band)
+
+    send_grads(range(chunks // 2, chunks))
     columns[:, :rows] = inputs[:, columns_of(dp_me)].T
     for j in range(1, dps):
         column_copy(j).wait_recv()
@@ -250,7 +265,7 @@
         for j in range(1, zs):
             z_copy(k, j).wait_recv()
             total = total + z_arrived[k, j].astype(f32)
-        sums[x_me, z_me, :, k * width : (k + 1) * width] = total.astype(jnp.bfloat16)
+        sums[x_me, z_me, :, lanes_of(k)] = total.astype(jnp.bfloat16)
         for j in range(1, zs):
             az_send_copy(k, j).start()
 
@@ -279,12 +294,23 @@
                 result[j] = total.astype(jnp.bfloat16)
                 result_copy(j).start()
 
-    for step in range(chunks + 3):
-        for stage, lag in ((first, 0), (second, 1), (third, 2), (fourth, 3)):
-            if 0 <= step - lag < chunks:
-                stage(step - lag)
+    middle = chunks // 2
+    for step in range(chunks + 2):
+        if step < chunks:
+            first(order(step))
+        if middle <= step < chunks:
+            second(order(step))
+        if middle < step <= chunks:
+            second(order(step - 1 - middle))
+            third(order(step - 1))
+        if middle + 1 < step:
+            third(order(step - 2 - middle))
+            fourth(order(step - 2))
         if step == chunks - 1:
             project()
+        if middle + 2 < step:
+            fourth(order(step - 3 - middle))
+    fourth(order(middle - 1))
     for k in range(chunks):
         for j in range(1, xs):
             ax_recv_copy(k, j).wait_recv()

time: 97 us -> 99.7 us (1.028)
  Pallas kernels: 90.8 us -> 93.4 us
    pallas_call x1, Pallas kernels: 90.8 us -> 93.4 us  [on_device(): pl.pallas_call(functools.partial(exchange_kernel, (dps, xs, zs, CHUNKS)),...]
where the time goes in v4:
time: 99.7 us; the launch traced here: 99.5 us
  Pallas kernels  93.4 us (94%)
  local copies, waits for them, and re-layouts  3.29 us (3%)
  other arithmetic  2.13 us (2%)
    pallas_call x1, Pallas kernels, on_device(): pl.pallas_call(functools.partial(exchange_kernel, (dps, xs, zs, CHUNKS)),...  93.4 us
    slice x1, local copies, waits for them, and re-layouts, on_device(): return (input_grad[None], weight_rows[:, :gated], weight_rows[:, gated:])  2.32 us
    mul x1, other arithmetic, on_device(): weight_rows = sums.reshape(own_columns, 2 * gated).astype(f32) * grad_scale  2.13 us

profile of v4, /device:TPU:0, one launch (start us, length us, event | category | flops | bytes accessed | tf_op | source)
XLA Modules:
  0.0 99.5 jit_solution(6733039172510696506)
XLA Ops:
  0.6 93.4 %shard_map.103 = (bf16[2,4,64,2048]{3,2,1,0:T(8,128)(2,1)}, bf16[256,2048]{1,0:T(8,128)(2,1)}) custom-call(bf16[256,2048]{1,0:T(8,128)(2,1)} %bitcast.9, bf16[256,1024]{1,0:T(8,128)(2,1)} %bitcast.10, bf16[256,1024]{1,0:T(8,128)(2,1)} %bitcast.11, bf16[256,1024]{1,0:T(8,128)(2,1)} %bitcast.12, f32[1,1024]{1,0:T(1,128)} %bitcast.13, ...), custom_call_target="tpu_custom_call" | custom-call | tf_op jit(solution)/shard_map/pallas_call | solution.py:351
  94.0 2.1 %convert_multiply_fusion = f32[2,4,64,2048]{3,2,1,0:T(8,128)S(1)} fusion(bf16[2,4,64,2048]{3,2,1,0:T(8,128)(2,1)} %get-tuple-element.6), kind=kLoop, calls=%fused_computation | loop fusion | flops 2097152 | bytes 6291456 | tf_op jit(solution)/shard_map/mul | solution.py:395
  96.2 0.0 copy-start
  96.2 2.3 %fusion = (f32[512,1024]{1,0:T(8,128)}, f32[512,1024]{1,0:T(8,128)}) fusion(f32[512,2048]{1,0:T(8,128)S(1)} %bitcast.7), kind=kLoop, calls=%fused_computation.1 | loop fusion | bytes 8388608 | tf_op jit(solution)/shard_map/slice | solution.py:396
  98.5 0.0 copy-done
  98.5 1.0 copy.12
Async XLA Ops:
  96.2 2.3 %copy-start = (bf16[256,2048]{1,0:T(8,128)(2,1)S(1)}, bf16[256,2048]{1,0:T(8,128)(2,1)}, u32[]{:S(2)}) copy-start(bf16[256,2048]{1,0:T(8,128)(2,1)} %get-tuple-element.5) | copy-start | bytes 3145732
